TPU v7x, 256 devices: a 4x2x16 block of a 4x16x16 slice. The times are simulated.
256 devices in a mesh: grp: 2 (over y), ep: 64 (over z, x), tp: 2 (over core).
Axes of the slice: x: 4, y: 2, z: 16, core: 2. Of those that a mesh axis runs over, the one named last changes fastest.
The devices are a block of a 4x16x16 slice.
Arguments:
- tokens: bfloat16 [16384, 2048], P(('grp', 'ep')), parts along dimension 0, may hold values from -6 to 6
- in_gain: float32 [2048], replicated, may hold values from 0.1 to 1.9
- routing: int32 [16384, 4], P(('grp', 'ep')), parts along dimension 0, may hold values from 0 to 127, as said below
- gate_prob: float32 [16384, 4], P(('grp', 'ep')), parts along dimension 0, may hold values from 0.05 to 1
- w_gate: bfloat16 [128, 2048, 512], P('ep', None, 'tp'), may hold values from -0.125 to 0.125
- w_up: bfloat16 [128, 2048, 512], P('ep', None, 'tp'), may hold values from -0.125 to 0.125
- w_down: bfloat16 [128, 512, 2048], P('ep', 'tp')
- out_gain: float32 [2048], P('tp'), may hold values from 0.1 to 1.9
Outputs:
- output: bfloat16 [16384, 2048], P(('grp', 'ep'), 'tp'), parts along dimension 0
There are 2 independent parts, one for each index of `grp`. A program takes and returns all parts, laid end to end along the dimension named above; an argument that names none is the same for every part. Nothing has to cross between parts.
Inputs may be any that keep to these rules, and one draw needn't show every extreme that they name: `routing`: each row names 4 different experts, all of one group (the same value of expert // 32). In the rows of one device no expert is named more than 8 times, and in every device's rows some expert is named exactly 8 times.
All inputs are finite; a program needn't handle non-finite values.
Results may differ from a plain program's by a relative error of at most 0.0077.
Values may be sent and summed in bfloat16 or wider, within the bound.
A program may use at most 64 MiB of HBM per device.

v0:
```python
import jax
import jax.numpy as jnp
from jax import lax
from jax.sharding import PartitionSpec as P

GROUPS = 4


EPS = 1e-06


def split_up(value, dim, peers):
    dims = value.shape
    tiles = value.reshape(*dims[:dim], peers, dims[dim] // peers, *dims[dim + 1 :])
    return jnp.moveaxis(tiles, dim, 0)


def sent_and_summed(value, axis, dim):
    tiles = split_up(value, dim, lax.axis_size(axis))
    arrived = lax.all_to_all(tiles, axis, split_axis=0, concat_axis=0, tiled=True)
    return arrived.astype(jnp.float32).sum(axis=0)


def gathered_total(value, axis):
    tiles = lax.all_gather(value, axis)
    return tiles.sum(axis=0)


def slot_ranks(flat_routes, expert_count):
    matches = (flat_routes[:, None] == jnp.arange(expert_count, dtype=jnp.int32)[None, :]).astype(
        jnp.int32
    )
    earlier = jnp.cumsum(matches, axis=0) - matches
    return jnp.sum(earlier * matches, axis=1)


def fill_rows(source, entries):
    filled = entries > 0
    return jnp.where(
        filled[:, None], source[jnp.maximum(entries - 1, 0)], jnp.zeros((), source.dtype)
    )


def body(tokens, in_gain, routing, gate_prob, w_gate, w_up, w_down, out_gain):
    ep_count = lax.axis_size("ep")
    local_experts = w_gate.shape[0]
    expert_count = local_experts * ep_count
    tok_dev, top_count = routing.shape
    model_width = tokens.shape[1]
    half_width = out_gain.shape[0]
    group_width = expert_count // GROUPS
    row_cap = max(2, tok_dev * top_count // (2 * group_width))
    floats = tokens.astype(jnp.float32)
    normed = (
        floats * lax.rsqrt(jnp.mean(floats * floats, axis=-1, keepdims=True) + EPS) * in_gain
    ).astype(jnp.bfloat16)
    flat_routes = routing.reshape(-1)
    slot_rank = slot_ranks(flat_routes, expert_count)
    slot_ids = flat_routes * row_cap + slot_rank
    token_ids = jnp.arange(tok_dev * top_count, dtype=jnp.int32) // top_count
    slot_table = jnp.zeros((expert_count * row_cap,), jnp.int32).at[slot_ids].set(token_ids + 1)
    own_columns = lax.dynamic_slice_in_dim(normed, lax.axis_index("tp") * half_width, half_width, 1)
    sendbuf = fill_rows(own_columns, slot_table).reshape(
        ep_count, local_experts, row_cap, half_width
    )
    arrived = lax.all_to_all(sendbuf, "ep", split_axis=0, concat_axis=0, tiled=True)
    arrived = lax.all_gather(arrived, "tp", axis=3, tiled=True)
    gate_act = jnp.einsum("secd,edf->secf", arrived, w_gate, preferred_element_type=jnp.float32)
    up_act = jnp.einsum("secd,edf->secf", arrived, w_up, preferred_element_type=jnp.float32)
    hidden = (jax.nn.silu(gate_act) * up_act).astype(jnp.bfloat16)
    partial_out = jnp.einsum("secf,efd->secd", hidden, w_down, preferred_element_type=jnp.float32)
    results = sent_and_summed(partial_out.astype(jnp.bfloat16), "tp", 3).astype(jnp.bfloat16)
    returned = lax.all_to_all(results, "ep", split_axis=0, concat_axis=0, tiled=True).reshape(
        expert_count * row_cap, half_width
    )
    picked = returned[slot_ids].astype(jnp.float32).reshape(tok_dev, top_count, half_width)
    mixed_rows = jnp.sum(picked * gate_prob[:, :, None], axis=1)
    squares = jnp.sum(mixed_rows * mixed_rows, axis=1)
    total_squares = gathered_total(squares, "tp")
    inv_rms = lax.rsqrt(total_squares / model_width + EPS)
    return (mixed_rows * inv_rms[:, None] * out_gain).astype(jnp.bfloat16)


def solution(mesh):
    placed = (
        P(("grp", "ep"), None),
        P(),
        P(("grp", "ep"), None),
        P(("grp", "ep"), None),
        P("ep", None, "tp"),
        P("ep", None, "tp"),
        P("ep", "tp", None),
        P("tp"),
    )
    return jax.shard_map(
        body, mesh=mesh, in_specs=placed, out_specs=P(("grp", "ep"), "tp"), check_vma=False
    )
```

profile of v0, /device:TPU:33, one launch (start us, length us, event | category | flops | bytes accessed | tf_op | source)
XLA Modules:
  0.0 331.5 jit_solution(8232878903041759823)
XLA Ops:
  6.6 1.3 convert_element_type.36
  7.9 1.2 multiply_reduce_fusion.1
  9.6 0.2 fusion.24
  10.1 0.2 fusion.23
  10.3 2.4 scatter_custom_fusion
  12.8 0.1 broadcast_in_dim.16
  13.1 5.4 %gather_fusion = bf16[1024,1024]{1,0:T(8,128)(2,1)} fusion(bf16[128,1024]{1,0:T(8,128)(2,1)S(1)} %fusion.20, s32[1024]{0:T(1024)S(1)} %maximum_clamp_fusion), kind=kCustom, calls=%fused_computation | custom fusion | bytes 4198400 | tf_op jit(solution)/shard_map/gather | solution.py:40
  18.5 1.8 broadcast_select_fusion
  20.3 124.6 %all_to_all.15 = bf16[64,2,8,1024]{3,2,1,0:T(8,128)(2,1)S(1)} all-to-all(bf16[64,2,8,1024]{3,2,1,0:T(8,128)(2,1)S(1)} %broadcast_select_fusion), channel_id=1, replica_groups=mesh['grp'=2,'ep'=64,'tp'=2] {'ep'}, dimensions={0} | all-to-all | bytes 4194304 | tf_op jit(solution)/shard_map/all_to_all | solution.py:66
  144.9 1.5 copy.33
  146.5 19.9 %all-gather.4.cloned.1.call-done = bf16[64,2,8,2048]{3,2,0,1:T(8,128)(2,1)} async-done(((bf16[64,2,8,1024]{3,2,0,1:T(8,128)(2,1)}), bf16[64,2,8,2048]{3,2,0,1:T(8,128)(2,1)}) %all-gather.4.cloned.1.call-update) | async-done | bytes 4194320 | tf_op jit(solution)/shard_map/all_gather | solution.py:67
  166.4 4.1 %fusion.5 = f32[64,2,8,256]{3,2,0,1:T(8,128)S(1)} fusion(bf16[64,2,8,2048]{3,2,0,1:T(8,128)(2,1)} %all-gather.4.cloned.1.call-done, bf16[2,2048,256]{2,1,0:T(8,128)(2,1)} %param.12), kind=kOutput, calls=%fused_computation.12 | convolution fusion | flops 1073741824 | bytes 7340032 | tf_op jit(solution)/shard_map/secd,edf->secf/dot_general | solution.py:68
  170.5 7.2 %convolution_convert_fusion = bf16[2,64,8,2048]{3,2,1,0:T(8,128)(2,1)} fusion(bf16[2,256,2048]{2,1,0:T(8,128)(2,1)S(1)} %copy-done, bf16[64,2,8,2048]{3,2,0,1:T(8,128)(2,1)} %all-gather.4.cloned.1.call-done, bf16[2,2048,256]{2,1,0:T(8,128)(2,1)} %param.13, f32[64,2,8,256]{3,2,0,1:T(8,128)S(1)} %fusion.5), kind=kOutput, calls=%fused_computation.4 | convolution fusion | flops 2151153664 | bytes 13631488 | tf_op jit(solution)/shard_map/secf,efd->secd/dot_general | solution.py:71
  177.7 2.6 copy.43
  180.4 8.0 %all_to_all.16 = bf16[2,64,2,8,1024]{4,3,1,2,0:T(8,128)(2,1)} all-to-all(bf16[2,64,2,8,1024]{4,3,1,2,0:T(8,128)(2,1)S(1)} %bitcast.61), channel_id=1, replica_groups=mesh['grp'=2,'ep'=64,'tp'=2] {'tp'}, dimensions={0} | all-to-all | bytes 8388608 | tf_op jit(solution)/shard_map/all_to_all | solution.py:20
  188.4 5.2 %reduce_sum.62 = bf16[64,2,8,1024]{3,2,0,1:T(8,128)(2,1)} reduce(bf16[2,64,2,8,1024]{4,3,1,2,0:T(8,128)(2,1)} %all_to_all.16, bf16[]{:T(256)} %constant.55.clone.1), dimensions={0}, to_apply=%region_5.6 | reduce | flops 1048576 | bytes 6291458 | tf_op jit(solution)/shard_map/reduce_sum | solution.py:21
  193.6 3.2 copy.36
  196.8 16.3 %all-to-all-start.2 = ((bf16[64,2,8,1024]{3,2,1,0:T(8,128)(2,1)}), bf16[64,2,8,1024]{3,2,1,0:T(8,128)(2,1)}, u32[]{:S(2)}, u32[]{:S(2)}) async-start(bf16[64,2,8,1024]{3,2,1,0:T(8,128)(2,1)} %copy.36), calls=%async_computation.2 | async-start | bytes 4194304 | tf_op jit(solution)/shard_map/all_to_all | solution.py:73
  213.2 95.1 %all-to-all-done.2 = bf16[64,2,8,1024]{3,2,1,0:T(8,128)(2,1)} async-done(((bf16[64,2,8,1024]{3,2,1,0:T(8,128)(2,1)}), bf16[64,2,8,1024]{3,2,1,0:T(8,128)(2,1)}, u32[]{:S(2)}, u32[]{:S(2)}) %all-to-all-start.2) | async-done | bytes 2097184 | tf_op jit(solution)/shard_map/all_to_all | solution.py:73
  308.3 4.6 %gather_fusion.1 = bf16[512,1024]{1,0:T(8,128)(2,1)S(1)} fusion(bf16[1024,1024]{1,0:T(8,128)(2,1)} %bitcast.17, s32[1024]{0:T(1024)S(1)} %pad_clamp_fusion), kind=kCustom, calls=%fused_computation.1 | custom fusion | bytes 2099200 | tf_op jit(solution)/shard_map/gather | solution.py:76
  312.9 1.7 reshape.83
  314.6 3.0 multiply_reduce_fusion
  317.7 6.1 %all-gather.1 = f32[2,1,128]{2,1,0:T(1,128)S(1)} all-gather(f32[1,1,128]{2,1,0:T(1,128)S(1)} %bitcast.70), channel_id=2, replica_groups=mesh['grp'=2,'ep'=64,'tp'=2] {'tp'}, dimensions={0}, use_global_device_ids=true | all-gather | bytes 1536 | tf_op jit(solution)/shard_map/all_gather | solution.py:25
  323.9 0.8 multiply_convert_fusion
  (37 shorter events, 1.2 us)
Async XLA Ops:
  6.5 164.0 %copy-start = (bf16[2,256,2048]{2,1,0:T(8,128)(2,1)S(1)}, bf16[2,256,2048]{2,1,0:T(8,128)(2,1)}, u32[]{:S(2)}) copy-start(bf16[2,256,2048]{2,1,0:T(8,128)(2,1)} %param.14) | copy-start | bytes 6291460
  6.6 2.5 copy-start.1
  6.6 159.8 %all-gather.4.cloned.1.call-start = ((), (), s32[]{:S(2)}) async-start(), calls=%async_computation.3 | async-start | bytes 6291456 | tf_op jit(solution)/shard_map/all_gather | solution.py:67
  6.6 6.4 %copy-start.4 = (f32[2048]{0:T(1024)S(1)}, f32[2048]{0:T(1024)}, u32[]{:S(2)}) copy-start(f32[2048]{0:T(1024)} %param.9) | copy-start | bytes 24580
  196.8 16.3 %copy-start.3 = (f32[128,4]{0,1:T(4,128)S(1)}, f32[128,4]{0,1:T(4,128)}, u32[]{:S(2)}) copy-start(f32[128,4]{0,1:T(4,128)} %param.11) | copy-start | bytes 6148
  196.8 111.5 %all-to-all-start.2 = ((bf16[64,2,8,1024]{3,2,1,0:T(8,128)(2,1)}), bf16[64,2,8,1024]{3,2,1,0:T(8,128)(2,1)}, u32[]{:S(2)}, u32[]{:S(2)}) async-start(bf16[64,2,8,1024]{3,2,1,0:T(8,128)(2,1)} %copy.36), calls=%async_computation.2 | async-start | bytes 4194304 | tf_op jit(solution)/shard_map/all_to_all | solution.py:73
  314.6 9.2 %copy-start.2 = (f32[1024]{0:T(1024)S(1)}, f32[1024]{0:T(1024)}, u32[]{:S(2)}) copy-start(f32[1024]{0:T(1024)} %param.15) | copy-start | bytes 12292
Sparse Core Ops, SparseCore 0:
  146.6 19.7 all-gather.3
where the time goes:
time: 332 us
  blocking collectives  139 us (42%)
  waiting for transfers between devices  115 us (35%)
  local copies, waits for them, and re-layouts  22.4 us (7%)
  starting transfers between devices  16.3 us (5%)
  other arithmetic  14.1 us (4%)
  between operations  13.6 us (4%)
  matrix products  11.3 us (3%)
    all_to_all x1, blocking collectives, body(): lax.all_to_all(sendbuf, 'ep', split_axis=0, concat_axis=0, tiled=True)  125 us
    all_to_all x1, waiting for transfers between devices, body(): lax.all_to_all(results, 'ep', split_axis=0, concat_axis=0, tiled=True)  95.1 us
    all_gather x1, waiting for transfers between devices, body(): arrived = lax.all_gather(arrived, 'tp', axis=3, tiled=True)  19.9 us
    all_to_all x1, starting transfers between devices, body(): lax.all_to_all(results, 'ep', split_axis=0, concat_axis=0, tiled=True)  16.3 us
    all_to_all x1, blocking collectives, sent_and_summed(): lax.all_to_all(tiles, axis, split_axis=0, concat_axis=0, tiled=True)  8.04 us
    dot_general x1, matrix products, body(): jnp.einsum('secf,efd->secd', hidden, w_down, preferred_element_type=jnp.f...  7.24 us
  transfers between devices with their start and end apart: 2, of which 2 were waited for; matrix products, arithmetic and copies ran while one was open for 0% of the time, Pallas kernels for 0%

commit v1 on v0

v1 whole, which is shorter than its diff:
```python
import functools
import math

import jax
import jax.numpy as jnp
from jax import lax
from jax.experimental import pallas as pl
from jax.experimental.pallas import tpu as pltpu
from jax.sharding import PartitionSpec as P

GROUPS = 4
EPS = 1e-06
MESH = pl.DeviceIdType.MESH
F32 = jnp.float32
BF16 = jnp.bfloat16
I32 = jnp.int32


def iota(shape, dim):
    return lax.broadcasted_iota(I32, shape, dim)


def mm(a, b):
    return jnp.dot(a, b, preferred_element_type=F32)


def mm_tn(a, b):
    return lax.dot_general(a, b, (((0,), (0,)), ((), ())), preferred_element_type=F32)


def kernel(
    cfg, routing, prob, tokens, gain, out_gain, wg_hbm, wu_hbm, wd_hbm, out_ref,
    wg, wu, wd, place, meta_out, meta_in, packed, zbuf, mix_hi, mix_lo, xsend, rows, hid,
    back_out, back_in, part, psend, rz, side, ret, own_part, sq_out, sq_in,
    w_sem, wd_send, wd_recv, m_send, m_recv, i_send, z_send, z_recv, x_send, x_recv,
    d_send, d_recv, h_send, h_recv, b_send, b_recv, p_send, c_recv, side_recv, ret_recv,
    q_send, q_recv,
):
    lines, side_len, tok, top, cap, gmax, half, width, epg = cfg
    cols, deep = side_len, side_len
    me = lax.axis_index("ep")
    core = lax.axis_index("tp")
    peer = 1 - core
    x, z = lax.rem(me, cols), lax.div(me, cols)
    grp, o = lax.div(z, deep), lax.rem(z, deep)
    late = lax.div(o, deep // 2)
    loc = wg.shape[0]

    def at_z(zz):
        return {"ep": zz * cols + x}

    def at_x(xx):
        return {"ep": z * cols + xx}

    def remote(src, dst, s, r, dev):
        return pltpu.make_async_remote_copy(
            src_ref=src, dst_ref=dst, send_sem=s, recv_sem=r, device_id=dev, device_id_type=MESH
        )

    other_core = {"tp": peer}
    my_cols = pl.ds(pl.multiple_of(core * half, half), half)
    peer_cols = pl.ds(pl.multiple_of(peer * half, half), half)

    barrier = pltpu.get_barrier_semaphore()
    for j in range(1, lines):
        pl.semaphore_signal(barrier, 1, device_id=at_z(lax.rem(z + j, lines)), device_id_type=MESH)
    for j in range(1, cols):
        pl.semaphore_signal(barrier, 1, device_id=at_x(lax.rem(x + j, cols)), device_id_type=MESH)
    pl.semaphore_signal(barrier, 1, device_id=other_core, device_id_type=MESH)

    w_copies = [
        pltpu.make_async_copy(wg_hbm, wg, w_sem.at[0]),
        pltpu.make_async_copy(wu_hbm, wu, w_sem.at[1]),
        pltpu.make_async_copy(wd_hbm.at[:, :, my_cols], wd.at[core], w_sem.at[2]),
    ]
    for copy in w_copies:
        copy.start()

    r_k = [routing[k : k + 1, :] for k in range(top)]
    g_t = lax.div(r_k[0], epg)
    experts = epg * GROUPS
    earlier = (iota((tok, tok), 0) < iota((tok, tok), 1)).astype(BF16)
    e_io = iota((experts, tok), 0)
    named = jnp.zeros((experts, tok), F32)
    for k in range(top):
        named = named + (e_io == r_k[k]).astype(F32)
    rank = mm(named.astype(BF16), earlier)
    g_io = iota((16, tok), 0)
    in_group = (g_io == g_t).astype(F32)
    g_rank = mm(in_group.astype(BF16), earlier)
    pos = jnp.sum(in_group * g_rank, axis=0, keepdims=True).astype(I32)
    for k in range(top):
        rank_k = jnp.sum(jnp.where(e_io == r_k[k], rank, 0.0), axis=0, keepdims=True)
        sq_out[k : k + 1, :] = ((r_k[k] - g_t * epg) * cap + 1).astype(F32) + rank_k
        sq_out[top + k : top + k + 1, :] = prob[k : k + 1, :]
    wide = 2 * gmax
    wr = iota((GROUPS * wide, tok), 0)
    sel2 = (wr == g_t * wide + pos) | (wr == g_t * wide + gmax + pos)
    meta = lax.dot_general(
        sq_out[0 : 2 * top, :], sel2.astype(F32), (((1,), (1,)), ((), ())),
        preferred_element_type=F32, precision=lax.Precision.HIGHEST,
    )
    for g in range(GROUPS):
        meta_out[g] = meta[:, g * wide : (g + 1) * wide]
    place[...] = (iota((GROUPS * gmax, tok), 0) == g_t * gmax + pos).astype(BF16)

    floats = tokens[...].astype(F32)
    inv = lax.rsqrt(jnp.mean(floats * floats, axis=-1, keepdims=True) + EPS)
    normed = (tokens[:, my_cols].astype(F32) * inv * gain[:, my_cols]).astype(BF16)
    packed[...] = mm(place[...], normed).astype(BF16).reshape(packed.shape)

    pl.semaphore_wait(barrier, (lines - 1) + (cols - 1) + 1)

    def rel(a):
        return lax.rem(a + 2 * GROUPS, GROUPS)

    def meta_copy(j):
        zt = lax.rem(z + j, lines)
        gt = lax.div(zt, deep)
        return remote(
            meta_out.at[gt], meta_in.at[rel(grp - gt), o], m_send.at[j], m_recv.at[j], at_z(zt)
        )

    for j in range(1, lines):
        meta_copy(j).start()

    def first(t, row):
        gt = lax.rem(grp + t, GROUPS)
        d = (GROUPS - t) % GROUPS
        return remote(
            packed.at[gt], zbuf.at[d, o], i_send.at[t], z_recv.at[d, o], at_z(gt * deep + row)
        )

    opp = first(2, (deep - 1) * (1 - late))
    nxt = first(1, 0)
    prv = first(3, deep - 1)
    own_up = remote(packed.at[grp], zbuf.at[0, o], i_send.at[0], z_recv.at[0, o], at_z(lax.rem(z + 1, lines)))
    own_dn = remote(packed.at[grp], zbuf.at[0, o], i_send.at[4], z_recv.at[0, o], at_z(lax.rem(z + lines - 1, lines)))
    opp.start()
    nxt.start()
    prv.start()
    pl.when(o < deep - 1)(own_up.start)
    pl.when(o > 0)(own_dn.start)
    wd_copy = remote(wd_hbm.at[:, :, peer_cols], wd.at[core], wd_send.at[0], wd_recv.at[0], other_core)
    wd_copy.start()
    zbuf[0, o] = packed[grp]
    meta_in[0, o] = meta_out[grp]

    def onward(plus):
        zz = lax.rem(z + plus * 2 - 1 + lines, lines)
        more = ((plus == 1) & (o < deep - 1)) | ((plus == 0) & (o > 0))
        return zz, more

    def z_copy(d, s, plus):
        zz, more = onward(plus)
        return remote(zbuf.at[d, s], zbuf.at[d, s], z_send.at[d, s], z_recv.at[d, s], at_z(zz)), more

    def arrive(d, s, plus):
        copy, more = z_copy(d, s, plus)
        copy.wait_recv()
        pl.when(more)(copy.start)

    d_near, d_far = 3 - 2 * late, 1 + 2 * late
    plus_near, plus_far = 1 - late, late
    half_deep = deep // 2

    def opp_item(j):
        s = lax.rem(j + half_deep * (1 - late), deep)
        return s, lax.div(s, half_deep)

    def own_item(j):
        s = lax.rem(o + j, deep)
        return s, (s < o).astype(I32)

    def arrive_opp(js):
        for j in js:
            s, plus = opp_item(j)
            arrive(2, s, plus)

    def arrive_side(d, plus):
        for s in range(deep):
            arrive(d, s, plus)

    def arrive_own():
        for j in range(1, deep):
            s, plus = own_item(j)
            arrive(0, s, plus)

    quad = deep * gmax
    piece = loc * deep * cap

    def x_copy(d, j):
        xx = lax.rem(x + j, cols)
        return remote(xsend.at[d, xx], rows.at[core, d, x], x_send.at[d, j], x_recv.at[d, j], at_x(xx))

    def x_arrival(d, j):
        xx = lax.rem(x + cols - j, cols)
        return remote(xsend.at[d, xx], rows.at[core, d, xx], x_send.at[d, j], x_recv.at[d, j], at_x(xx))

    def d_copy(d, j):
        xx = lax.rem(x + cols - j, cols)
        return remote(rows.at[core, d, xx], rows.at[core, d, xx], d_send.at[d, j], d_recv.at[d, j], other_core)

    def d_arrival(d, j):
        xx = lax.rem(x + cols - j, cols)
        return remote(rows.at[peer, d, xx], rows.at[peer, d, xx], d_send.at[d, j], d_recv.at[d, j], other_core)

    def select(d):
        lane = iota((2 * top, wide), 1)
        pairs = [
            jnp.where(lane < gmax, meta_in[d, 2 * i], meta_in[d, 2 * i + 1]) for i in range(deep // 2)
        ]
        info = jnp.concatenate(pairs, axis=1)
        zs = lax.div(iota((1, quad), 1), gmax)
        s_io = iota((quad, quad), 0)
        a = jnp.zeros((quad, quad), F32)
        w = jnp.zeros((quad, quad), F32)
        span = cols * loc * cap
        for k in range(top):
            v = info[k : k + 1, :].astype(I32) - 1 - span * o
            ok = (v >= 0) & (v < span)
            sid = jnp.where(ok, lax.div(v, cap) * (deep * cap) + zs * cap + lax.rem(v, cap), -1)
            hit = s_io == sid
            a = jnp.where(hit, 1.0, a)
            w = jnp.where(hit, info[top + k : top + k + 1, :], w)
        hi = w.astype(BF16)
        mix_hi[d] = hi
        mix_lo[d] = (w - hi.astype(F32)).astype(BF16)
        picked = mm(a.astype(BF16), zbuf[d].reshape(quad, half)).astype(BF16)
        xsend[d] = picked.reshape(cols, piece, half)
        for j in range(1, cols):
            x_copy(d, j).start()
        rows[core, d, x] = xsend[d, x]
        d_copy(d, 0).start()

    def exchange(d):
        for j in range(1, cols):
            x_arrival(d, j).wait_recv()
            d_copy(d, j).start()

    m = cols * deep * cap
    ff = wg.shape[2]

    def h_copy(d):
        return remote(hid.at[core, d], hid.at[core, d], h_send.at[d], h_recv.at[d], other_core)

    def h_arrival(d):
        return remote(hid.at[peer, d], hid.at[peer, d], h_send.at[d], h_recv.at[d], other_core)

    def gate_up(d):
        for j in range(cols):
            d_arrival(d, j).wait_recv()
        for e in range(loc):
            r = [
                rows[h, d, :, e * deep * cap : (e + 1) * deep * cap, :].reshape(m, half) for h in range(2)
            ]
            ga = mm(r[0], wg[e, :half, :]) + mm(r[1], wg[e, half:, :])
            up = mm(r[0], wu[e, :half, :]) + mm(r[1], wu[e, half:, :])
            hid[core, d, e] = (ga / (1.0 + jnp.exp(-ga)) * up).astype(BF16)
        h_copy(d).start()

    def b_copy(d, j):
        xx = lax.rem(x + j, cols)
        return remote(back_out.at[d, xx], back_in.at[d, x], b_send.at[d, j], b_recv.at[d, j], at_x(xx))

    def b_arrival(d, j):
        xx = lax.rem(x + cols - j, cols)
        return remote(back_out.at[d, xx], back_in.at[d, xx], b_send.at[d, j], b_recv.at[d, j], at_x(xx))

    def down(d):
        h_arrival(d).wait_recv()
        for e in range(loc):
            y = mm(hid[0, d, e], wd[0, e]) + mm(hid[1, d, e], wd[1, e])
            back_out[d, :, e * deep * cap : (e + 1) * deep * cap, :] = y.astype(BF16).reshape(
                cols, deep * cap, half
            )
        for j in range(1, cols):
            b_copy(d, j).start()
        back_in[d, x] = back_out[d, x]

    def home_copy(d, s, plus):
        direct = jnp.where(plus == 1, 0, deep - 1)
        gs = lax.rem(grp + d, GROUPS)
        return remote(
            psend.at[d, s], ret.at[grp], p_send.at[d, s], ret_recv.at[lax.rem(GROUPS - d, GROUPS)],
            at_z(gs * deep + s),
        ), o == direct

    def chain_copy(d, s, plus):
        zz = lax.rem(z - (plus * 2 - 1) + lines, lines)
        return remote(psend.at[d, s], rz.at[d, s], p_send.at[d, s], c_recv.at[d, s], at_z(zz))

    def side_copy(s, plus):
        zz = lax.rem(z - (plus * 2 - 1) + lines, lines)
        return remote(psend.at[0, s], side.at[1 - plus], p_send.at[0, s], side_recv.at[1 - plus], at_z(zz))

    def add_up(d, s, plus):
        _, more = onward(plus)
        mine = pl.ds(s * gmax, gmax)

        @pl.when(more)
        def _():
            chain_copy(d, s, plus).wait_recv()
            psend[d, s] = (part[mine, :] + rz[d, s].astype(F32)).astype(BF16)

        @pl.when(jnp.logical_not(more))
        def _():
            psend[d, s] = part[mine, :].astype(BF16)

    def combine(d):
        for j in range(1, cols):
            b_arrival(d, j).wait_recv()
        res = back_in[d].reshape(quad, half)
        part[...] = mm_tn(mix_hi[d], res) + mm_tn(mix_lo[d], res)

    def send_far(d, s, plus):
        add_up(d, s, plus)
        home, last = home_copy(d, s, plus)
        pl.when(last)(home.start)
        pl.when(jnp.logical_not(last))(chain_copy(d, s, plus).start)

    def far_opp(j):
        s = lax.rem(j + half_deep * late, deep)
        return s, lax.div(s, half_deep)

    def combine_opp():
        combine(2)
        for j in range(deep):
            s, plus = far_opp(j)
            send_far(2, s, plus)

    def combine_side(d, plus):
        combine(d)
        for s in range(deep):
            send_far(d, s, plus)

    def own_order(j):
        s = late * j + (1 - late) * (deep - 1 - j)
        return s, (s < o).astype(I32)

    def combine_own():
        combine(0)
        for j in range(deep):
            s, plus = own_order(j)

            @pl.when(s == o)
            def _():
                own_part[...] = part[pl.ds(s * gmax, gmax), :]

            @pl.when(s != o)
            def _():
                add_up(0, s, plus)
                near = s + plus * 2 - 1 == o
                pl.when(near)(side_copy(s, plus).start)
                pl.when(jnp.logical_not(near))(chain_copy(0, s, plus).start)

    arrive_opp(range(deep))
    for j in range(1, lines):
        meta_copy(j).wait_recv()
    select(2)
    arrive_side(d_near, plus_near)
    select(d_near)
    exchange(2)
    w_copies[0].wait()
    w_copies[1].wait()
    gate_up(2)
    arrive_side(d_far, plus_far)
    select(d_far)
    exchange(d_near)
    w_copies[2].wait()
    wd_arrival = remote(wd_hbm.at[:, :, my_cols], wd.at[peer], wd_send.at[0], wd_recv.at[0], other_core)
    wd_arrival.wait_recv()
    down(2)
    gate_up(d_near)
    arrive_own()
    select(0)
    exchange(d_far)
    down(d_near)
    gate_up(d_far)
    exchange(0)
    down(d_far)
    combine_opp()
    gate_up(0)
    combine_side(d_far, plus_far)
    down(0)
    combine_side(d_near, plus_near)
    combine_own()

    for t in range(1, GROUPS):
        gt = lax.rem(grp + t, GROUPS)
        remote(psend.at[t, o], ret.at[gt], p_send.at[t, o], ret_recv.at[t], at_z(z)).wait_recv()

    @pl.when(o < deep - 1)
    def _():
        side_copy(o, 1).wait_recv()
        own_part[...] += side[0].astype(F32)

    @pl.when(o > 0)
    def _():
        side_copy(o, 0).wait_recv()
        own_part[...] += side[1].astype(F32)

    ret[grp] = own_part[...].astype(BF16)
    mixed = mm_tn(place[...], ret[...].reshape(GROUPS * gmax, half))
    sq = jnp.zeros((tok, 128), F32)
    for i in range(half // 128):
        v = mixed[:, i * 128 : (i + 1) * 128]
        sq = sq + v * v
    sq_out[...] = sq
    q_copy = remote(sq_out, sq_in, q_send.at[0], q_recv.at[0], other_core)
    q_copy.start()
    q_copy.wait_recv()
    total = jnp.sum(sq_out[...] + sq_in[...], axis=1, keepdims=True)
    out_ref[...] = (mixed * lax.rsqrt(total / width + EPS) * out_gain[...]).astype(BF16)

    q_copy.wait_send()
    for j in range(1, lines):
        meta_copy(j).wait_send()
    opp.wait_send()
    nxt.wait_send()
    prv.wait_send()
    pl.when(o < deep - 1)(own_up.wait_send)
    pl.when(o > 0)(own_dn.wait_send)
    wd_copy.wait_send()

    def sent(d, s, plus):
        copy, more = z_copy(d, s, plus)
        pl.when(more)(copy.wait_send)
        chain_copy(d, s, plus).wait_send()

    for s in range(deep):
        sent(2, s, s // half_deep)
        sent(3, s, 1)
        sent(1, s, 0)
    for j in range(1, deep):
        s, plus = own_item(j)
        sent(0, s, plus)
    for d in range(GROUPS):
        h_copy(d).wait_send()
        d_copy(d, 0).wait_send()
        for j in range(1, cols):
            d_copy(d, j).wait_send()
            x_copy(d, j).wait_send()
            b_copy(d, j).wait_send()


def body(tokens, in_gain, routing, gate_prob, w_gate, w_up, w_down, out_gain):
    ep_count = lax.axis_size("ep")
    loc, width, ff = w_gate.shape
    tok, top = routing.shape
    half = out_gain.shape[0]
    epg = loc * ep_count // GROUPS
    cap = max(2, tok * top // (2 * epg))
    gmax = epg * cap // top
    side = math.isqrt(ep_count // GROUPS)
    lines = ep_count // side
    cols, deep = side, side
    quad = deep * gmax
    piece = loc * deep * cap
    m = cols * deep * cap
    cfg = (lines, side, tok, top, cap, gmax, half, width, epg)
    vmem = pl.BlockSpec(memory_space=pltpu.VMEM)
    anyw = pl.BlockSpec(memory_space=pl.ANY)
    dma = pltpu.SemaphoreType.DMA
    scratch = [
        pltpu.VMEM(w_gate.shape, BF16),
        pltpu.VMEM(w_up.shape, BF16),
        pltpu.VMEM((2, loc, ff, half), BF16),
        pltpu.VMEM((GROUPS * gmax, tok), BF16),
        pltpu.VMEM((GROUPS, 2 * top, 2 * gmax), F32),
        pltpu.VMEM((GROUPS, deep, 2 * top, 2 * gmax), F32),
        pltpu.VMEM((GROUPS, gmax, half), BF16),
        pltpu.VMEM((GROUPS, deep, gmax, half), BF16),
        pltpu.VMEM((GROUPS, quad, quad), BF16),
        pltpu.VMEM((GROUPS, quad, quad), BF16),
        pltpu.VMEM((GROUPS, cols, piece, half), BF16),
        pltpu.VMEM((2, GROUPS, cols, piece, half), BF16),
        pltpu.VMEM((2, GROUPS, loc, m, ff), BF16),
        pltpu.VMEM((GROUPS, cols, piece, half), BF16),
        pltpu.VMEM((GROUPS, cols, piece, half), BF16),
        pltpu.VMEM((quad, half), F32),
        pltpu.VMEM((GROUPS, deep, gmax, half), BF16),
        pltpu.VMEM((GROUPS, deep, gmax, half), BF16),
        pltpu.VMEM((2, gmax, half), BF16),
        pltpu.VMEM((GROUPS, gmax, half), BF16),
        pltpu.VMEM((gmax, half), F32),
        pltpu.VMEM((tok, 128), F32),
        pltpu.VMEM((tok, 128), F32),
        dma((3,)),
        dma((1,)),
        dma((1,)),
        dma((lines,)),
        dma((lines,)),
        dma((5,)),
        dma((GROUPS, deep)),
        dma((GROUPS, deep)),
        dma((GROUPS, cols)),
        dma((GROUPS, cols)),
        dma((GROUPS, cols)),
        dma((GROUPS, cols)),
        dma((GROUPS,)),
        dma((GROUPS,)),
        dma((GROUPS, cols)),
        dma((GROUPS, cols)),
        dma((GROUPS, deep)),
        dma((GROUPS, deep)),
        dma((2,)),
        dma((GROUPS,)),
        dma((1,)),
        dma((1,)),
    ]
    return pl.pallas_call(
        functools.partial(kernel, cfg),
        out_shape=jax.ShapeDtypeStruct((tok, half), BF16),
        in_specs=[vmem] * 5 + [anyw] * 3,
        out_specs=vmem,
        scratch_shapes=scratch,
        compiler_params=pltpu.CompilerParams(
            collective_id=0, has_side_effects=True, vmem_limit_bytes=60 * 1024 * 1024
        ),
    )(
        routing.T, gate_prob.T, tokens, in_gain.reshape(1, width), out_gain.reshape(1, half),
        w_gate, w_up, w_down,
    )


def solution(mesh):
    placed = (
        P(("grp", "ep"), None),
        P(),
        P(("grp", "ep"), None),
        P(("grp", "ep"), None),
        P("ep", None, "tp"),
        P("ep", None, "tp"),
        P("ep", "tp", None),
        P("tp"),
    )
    return jax.shard_map(
        body, mesh=mesh, in_specs=placed, out_specs=P(("grp", "ep"), "tp"), check_vma=False
    )
```

time: 332 us -> 193 us (0.58)
  Pallas kernels: 0 us -> 191 us
  blocking collectives: 139 us -> 0 us
  waiting for transfers between devices: 115 us -> 0 us
  local copies, waits for them, and re-layouts: 22.4 us -> 1.67 us
  starting transfers between devices: 16.3 us -> 0 us
  other arithmetic: 14.1 us -> 0 us
  between operations: 13.6 us -> 0.01 us
  matrix products: 11.3 us -> 0 us
    pallas_call x0 -> x1, Pallas kernels: none -> 191 us  [body(): pl.pallas_call(functools.partial(kernel, cfg), out_shape=jax.ShapeDtypeSt...]
    all_to_all x2 -> x0, blocking collectives: 133 us -> none  [the longest x1 125 us: body(): lax.all_to_all(sendbuf, 'ep', split_axis=0, concat_axis=0, tiled=True)]
    all_to_all x1 -> x0, waiting for transfers between devices: 95.1 us -> none  [body(): lax.all_to_all(results, 'ep', split_axis=0, concat_axis=0, tiled=True)]
    all_gather x1 -> x0, waiting for transfers between devices: 19.9 us -> none  [body(): arrived = lax.all_gather(arrived, 'tp', axis=3, tiled=True)]
    all_to_all x1 -> x0, starting transfers between devices: 16.3 us -> none  [body(): lax.all_to_all(results, 'ep', split_axis=0, concat_axis=0, tiled=True)]
    dot_general x2 -> x0, matrix products: 11.4 us -> none  [the longest x1 7.24 us: body(): jnp.einsum('secf,efd->secd', hidden, w_down, preferred_element_type=jnp.f...]
    gather x2 -> x0, local copies, waits for them, and re-layouts: 9.95 us -> none  [the longest x1 5.36 us: fill_rows(): source[jnp.maximum(entries - 1, 0)]]
    reduce_sum x6 -> x0, other arithmetic: 9.75 us -> none  [the longest x1 5.17 us: sent_and_summed(): return arrived.astype(jnp.float32).sum(axis=0)]
  transfers between devices with their start and end apart: 2 -> 0, of which waited for: 2 -> 0; matrix products, arithmetic and copies ran while one was open for 0% -> 0% of each run, Pallas kernels for 0% -> 0%
where the time goes in v1:
time: 193 us
  Pallas kernels  191 us (99%)
    pallas_call x1, Pallas kernels, body(): pl.pallas_call(functools.partial(kernel, cfg), out_shape=jax.ShapeDtypeSt...  191 us

profile of v1, /device:TPU:33, one launch (start us, length us, event | category | flops | bytes accessed | tf_op | source)
XLA Modules:
  0.0 192.9 jit_solution(6162057099140501111)
XLA Ops:
  0.0 191.2 %shard_map.82 = bf16[128,1024]{1,0:T(8,128)(2,1)} custom-call(s32[4,128]{1,0:T(4,128)} %bitcast.6, f32[4,128]{1,0:T(4,128)} %bitcast.7, bf16[128,2048]{1,0:T(8,128)(2,1)} %tokens.1, f32[1,2048]{1,0:T(1,128)} %bitcast.4, f32[1,1024]{1,0:T(1,128)} %bitcast.5, bf16[2,2048,256]{2,1,0:T(8,128)(2,1)} %wg_hbm.1, bf16[2,2048,256]{2,1,0:T(8,128)(2,1)} %wu_hbm.1, ...), custom_call_target="tpu_custom_call" | custom-call | tf_op jit(solution)/shard_map/pallas_call | solution.py:512
  191.2 1.7 copy.10

commit v2 on v1

v2 whole, which is shorter than its diff:
```python
import functools
import math

import jax
import jax.numpy as jnp
from jax import lax
from jax.experimental import pallas as pl
from jax.experimental.pallas import tpu as pltpu
from jax.sharding import PartitionSpec as P

GROUPS = 4
EPS = 1e-06
MESH = pl.DeviceIdType.MESH
F32 = jnp.float32
BF16 = jnp.bfloat16
I32 = jnp.int32


def iota(shape, dim):
    return lax.broadcasted_iota(I32, shape, dim)


def mm(a, b):
    return jnp.dot(a, b, preferred_element_type=F32)


def mm_tn(a, b):
    return lax.dot_general(a, b, (((0,), (0,)), ((), ())), preferred_element_type=F32)


ARRIVE, BACK, SELECT, EXCHANGE, GATE_UP, DOWN, COMBINE, SEND_OPP, WAIT_META, WAIT_W = range(10)

PLAN = (
    (ARRIVE, 0, 1, 0, 2), (ARRIVE, 3, 3, 0, 0), (WAIT_META, 0, 0, 0, 0), (SELECT, 0, 0, 0, 0),
    (EXCHANGE, 0, 0, 0, 0), (WAIT_W, 0, 0, 0, 0), (GATE_UP, 0, 0, 0, 0), (DOWN, 0, 0, 0, 0),
    (ARRIVE, 3, 2, 3, 3), (ARRIVE, 3, 1, 0, 3), (SELECT, 3, 1, 0, 1), (SEND_OPP, 0, 0, 0, 0),
    (ARRIVE, 3, 0, 3, 2), (SELECT, 3, 0, 3, 1), (COMBINE, 0, 0, 0, 0), (EXCHANGE, 3, 1, 0, 1),
    (GATE_UP, 3, 1, 0, 1), (DOWN, 3, 1, 0, 1), (ARRIVE, 0, 2, 3, 1), (ARRIVE, 0, 3, 1, 0),
    (EXCHANGE, 3, 0, 3, 1), (GATE_UP, 3, 0, 3, 1), (DOWN, 3, 0, 3, 1), (ARRIVE, 2, 3, 1, 1),
    (SELECT, 0, 1, 1, 0), (COMBINE, 3, 1, 0, 1), (ARRIVE, 1, 0, 3, 0), (ARRIVE, 2, 2, 1, 2),
    (SELECT, 2, 1, 3, 0), (COMBINE, 3, 0, 3, 1), (ARRIVE, 1, 1, 1, 3), (ARRIVE, 1, 2, 2, 3),
    (EXCHANGE, 0, 1, 1, 0), (SELECT, 1, 0, 1, 1), (ARRIVE, 1, 3, 2, 2), (SELECT, 1, 1, 2, 1),
    (GATE_UP, 0, 1, 1, 0), (ARRIVE, 2, 0, 2, 0), (EXCHANGE, 2, 1, 3, 0), (DOWN, 0, 1, 1, 0),
    (ARRIVE, 2, 1, 2, 1), (SELECT, 2, 0, 2, 0), (EXCHANGE, 1, 0, 1, 1), (GATE_UP, 1, 0, 3, 0),
    (EXCHANGE, 1, 1, 2, 1), (GATE_UP, 2, 1, 1, 1), (DOWN, 2, 1, 3, 0), (BACK, 0, 1, 0, 2),
    (DOWN, 1, 0, 1, 1), (GATE_UP, 1, 1, 2, 1), (COMBINE, 0, 1, 1, 0), (BACK, 0, 2, 0, 3),
    (BACK, 0, 3, 0, 0), (DOWN, 1, 1, 2, 1), (EXCHANGE, 2, 0, 2, 0), (COMBINE, 1, 0, 1, 1),
    (BACK, 1, 1, 1, 1), (GATE_UP, 2, 0, 2, 0), (BACK, 1, 0, 1, 0), (DOWN, 2, 0, 2, 0),
    (COMBINE, 2, 1, 2, 1), (COMBINE, 1, 1, 3, 0), (BACK, 1, 3, 3, 2), (BACK, 1, 2, 1, 3),
    (COMBINE, 2, 0, 2, 0), (BACK, 2, 0, 3, 3), (BACK, 2, 1, 1, 2), (BACK, 3, 2, 3, 0),
    (BACK, 3, 3, 2, 0), (BACK, 3, 0, 3, 1), (BACK, 3, 1, 2, 1), (BACK, 2, 2, 2, 2),
    (BACK, 2, 3, 2, 3),
)


def kernel(
    cfg, routing, prob, tokens, gain, out_gain, wg_hbm, wu_hbm, wd_hbm, out_ref,
    wg, wu, wd, place, meta_out, meta_in, packed, zbuf, mix_hi, mix_lo, xsend, rows, hid,
    back_out, back_in, part, psend, rz, side, ret, sq_out, sq_in,
    w_sem, wd_send, wd_recv, m_send, m_recv, i_send, z_send, z_recv, x_send, x_recv,
    d_send, d_recv, h_send, h_recv, b_send, b_recv, p_send, c_recv, side_recv, ret_recv,
    q_send, q_recv,
):
    lines, side_len, tok, top, cap, gmax, half, width, epg = cfg
    cols, deep = side_len, side_len
    two = deep // 2
    me = lax.axis_index("ep")
    core = lax.axis_index("tp")
    peer = 1 - core
    x, z = lax.rem(me, cols), lax.div(me, cols)
    grp, o = lax.div(z, deep), lax.rem(z, deep)
    late = lax.div(o, two)
    in_row = [(o == r).astype(I32) for r in range(deep)]
    loc = wg.shape[0]

    def at_z(zz):
        return {"ep": zz * cols + x}

    def at_x(xx):
        return {"ep": z * cols + xx}

    def remote(src, dst, s, r, dev):
        return pltpu.make_async_remote_copy(
            src_ref=src, dst_ref=dst, send_sem=s, recv_sem=r, device_id=dev, device_id_type=MESH
        )

    other_core = {"tp": peer}
    my_cols = pl.ds(pl.multiple_of(core * half, half), half)
    peer_cols = pl.ds(pl.multiple_of(peer * half, half), half)

    barrier = pltpu.get_barrier_semaphore()
    for j in range(1, lines):
        pl.semaphore_signal(barrier, 1, device_id=at_z(lax.rem(z + j, lines)), device_id_type=MESH)
    for j in range(1, cols):
        pl.semaphore_signal(barrier, 1, device_id=at_x(lax.rem(x + j, cols)), device_id_type=MESH)
    pl.semaphore_signal(barrier, 1, device_id=other_core, device_id_type=MESH)

    w_copies = [
        pltpu.make_async_copy(wg_hbm, wg, w_sem.at[0]),
        pltpu.make_async_copy(wu_hbm, wu, w_sem.at[1]),
        pltpu.make_async_copy(wd_hbm.at[:, :, my_cols], wd.at[core], w_sem.at[2]),
    ]
    for copy in w_copies:
        copy.start()

    r_k = [routing[k : k + 1, :] for k in range(top)]
    g_t = lax.div(r_k[0], epg)
    experts = epg * GROUPS
    earlier = (iota((tok, tok), 0) < iota((tok, tok), 1)).astype(BF16)
    e_io = iota((experts, tok), 0)
    named = jnp.zeros((experts, tok), F32)
    for k in range(top):
        named = named + (e_io == r_k[k]).astype(F32)
    rank = mm(named.astype(BF16), earlier)
    g_io = iota((16, tok), 0)
    in_group = (g_io == g_t).astype(F32)
    g_rank = mm(in_group.astype(BF16), earlier)
    pos = jnp.sum(in_group * g_rank, axis=0, keepdims=True).astype(I32)
    for k in range(top):
        rank_k = jnp.sum(jnp.where(e_io == r_k[k], rank, 0.0), axis=0, keepdims=True)
        sq_out[k : k + 1, :] = ((r_k[k] - g_t * epg) * cap + 1).astype(F32) + rank_k
        sq_out[top + k : top + k + 1, :] = prob[k : k + 1, :]
    wide = 2 * gmax
    wr = iota((GROUPS * wide, tok), 0)
    sel2 = (wr == g_t * wide + pos) | (wr == g_t * wide + gmax + pos)
    meta = lax.dot_general(
        sq_out[0 : 2 * top, :], sel2.astype(F32), (((1,), (1,)), ((), ())),
        preferred_element_type=F32, precision=lax.Precision.HIGHEST,
    )
    for g in range(GROUPS):
        meta_out[g] = meta[:, g * wide : (g + 1) * wide]
    place[...] = (iota((GROUPS * gmax, tok), 0) == g_t * gmax + pos).astype(BF16)

    floats = tokens[...].astype(F32)
    inv = lax.rsqrt(jnp.mean(floats * floats, axis=-1, keepdims=True) + EPS)
    normed = (tokens[:, my_cols].astype(F32) * inv * gain[:, my_cols]).astype(BF16)
    packed[...] = mm(place[...], normed).astype(BF16).reshape(packed.shape)

    pl.semaphore_wait(barrier, (lines - 1) + (cols - 1) + 1)

    def rel(a):
        return lax.rem(a + 2 * GROUPS, GROUPS)

    def meta_copy(j):
        zt = lax.rem(z + j, lines)
        gt = lax.div(zt, deep)
        return remote(
            meta_out.at[gt], meta_in.at[rel(grp - gt), o], m_send.at[j], m_recv.at[j], at_z(zt)
        )

    for j in range(1, lines):
        meta_copy(j).start()

    def chunk(d, s):
        return zbuf.at[d, lax.div(s, two), lax.rem(s, two)]

    def first(t, row):
        gt = lax.rem(grp + t, GROUPS)
        d = (GROUPS - t) % GROUPS
        return remote(
            packed.at[gt], chunk(d, o), i_send.at[t], z_recv.at[d, o], at_z(gt * deep + row)
        )

    opp = first(2, (deep - 1) * (1 - late))
    nxt = first(1, 0)
    prv = first(3, deep - 1)
    own_up = remote(packed.at[grp], chunk(0, o), i_send.at[0], z_recv.at[0, o], at_z(lax.rem(z + 1, lines)))
    own_dn = remote(packed.at[grp], chunk(0, o), i_send.at[4], z_recv.at[0, o], at_z(lax.rem(z + lines - 1, lines)))
    pl.when(o < deep - 1)(own_up.start)
    pl.when(o > 0)(own_dn.start)
    nxt.start()
    prv.start()
    wd_copy = remote(wd_hbm.at[:, :, peer_cols], wd.at[core], wd_send.at[0], wd_recv.at[0], other_core)
    wd_copy.start()
    zbuf[0, late, lax.rem(o, two)] = packed[grp]
    meta_in[0, o] = meta_out[grp]

    def onward(plus):
        zz = lax.rem(z + plus * 2 - 1 + lines, lines)
        more = ((plus == 1) & (o < deep - 1)) | ((plus == 0) & (o > 0))
        return zz, more

    def z_copy(d, s, plus):
        zz, more = onward(plus)
        return remote(chunk(d, s), chunk(d, s), z_send.at[d, s], z_recv.at[d, s], at_z(zz)), more

    def arrive(d, s, plus):
        copy, more = z_copy(d, s, plus)
        copy.wait_recv()
        pl.when(more)(copy.start)

    pair = two * gmax
    run = two * cap

    def x_to(src, dst, send, recv, d, h, j):
        xx = lax.rem(x + j, cols)
        return remote(src.at[d, h, xx], dst.at[d, h, x], send.at[d, h, j], recv.at[d, h, j], at_x(xx))

    def x_from(src, dst, send, recv, d, h, j):
        xx = lax.rem(x + cols - j, cols)
        return remote(src.at[d, h, xx], dst.at[d, h, xx], send.at[d, h, j], recv.at[d, h, j], at_x(xx))

    out_args = (xsend, rows.at[core], x_send, x_recv)
    back_args = (back_out, back_in, b_send, b_recv)
    x_order = [1, cols - 1] + list(range(2, cols - 1))

    def d_copy(d, h):
        return remote(rows.at[core, d, h], rows.at[core, d, h], d_send.at[d, h], d_recv.at[d, h], other_core)

    def d_arrival(d, h):
        return remote(rows.at[peer, d, h], rows.at[peer, d, h], d_send.at[d, h], d_recv.at[d, h], other_core)

    def select(d, h):
        lane = iota((2 * top, 2 * gmax), 1)
        info = jnp.where(lane < gmax, meta_in[d, two * h], meta_in[d, two * h + 1])
        zs = lax.div(iota((1, pair), 1), gmax)
        s_io = iota((pair, pair), 0)
        a = jnp.zeros((pair, pair), F32)
        w = jnp.zeros((pair, pair), F32)
        span = cols * loc * cap
        for k in range(top):
            v = info[k : k + 1, :].astype(I32) - 1 - span * o
            ok = (v >= 0) & (v < span)
            sid = jnp.where(ok, lax.div(v, cap) * run + zs * cap + lax.rem(v, cap), -1)
            hit = s_io == sid
            a = jnp.where(hit, 1.0, a)
            w = jnp.where(hit, info[top + k : top + k + 1, :], w)
        picked = mm(a.astype(BF16), zbuf[d, h].reshape(pair, half)).astype(BF16)
        xsend[d, h] = picked.reshape(cols, loc * run, half)
        for j in x_order:
            x_to(*out_args, d, h, j).start()
        rows[core, d, h, x] = xsend[d, h, x]
        hi = w.astype(BF16)
        mix_hi[d, h] = hi
        mix_lo[d, h] = (w - hi.astype(F32)).astype(BF16)

    def exchange(d, h):
        for j in x_order:
            x_from(*out_args, d, h, j).wait_recv()
        d_copy(d, h).start()

    m = cols * run

    def h_copy(d, h):
        return remote(hid.at[core, d, h], hid.at[core, d, h], h_send.at[d, h], h_recv.at[d, h], other_core)

    def h_arrival(d, h):
        return remote(hid.at[peer, d, h], hid.at[peer, d, h], h_send.at[d, h], h_recv.at[d, h], other_core)

    def gate_up(d, h):
        d_arrival(d, h).wait_recv()
        for e in range(loc):
            r = [rows[c, d, h, :, e * run : (e + 1) * run, :].reshape(m, half) for c in range(2)]
            ga = mm(r[0], wg[e, :half, :]) + mm(r[1], wg[e, half:, :])
            up = mm(r[0], wu[e, :half, :]) + mm(r[1], wu[e, half:, :])
            hid[core, d, h, e] = (ga / (1.0 + jnp.exp(-ga)) * up).astype(BF16)
        h_copy(d, h).start()

    def down(d, h):
        h_arrival(d, h).wait_recv()
        for e in range(loc):
            y = mm(hid[0, d, h, e], wd[0, e]) + mm(hid[1, d, h, e], wd[1, e])
            back_out[d, h, :, e * run : (e + 1) * run, :] = y.astype(BF16).reshape(cols, run, half)
        for j in x_order:
            x_to(*back_args, d, h, j).start()
        back_in[d, h, x] = back_out[d, h, x]

    def combine(d, h):
        for j in x_order:
            x_from(*back_args, d, h, j).wait_recv()
        res = back_in[d, h].reshape(pair, half)
        part[d, h] = mm_tn(mix_hi[d, h], res) + mm_tn(mix_lo[d, h], res)

    def home_copy(d, s, plus):
        direct = (deep - 1) * (1 - plus)
        gs = lax.rem(grp + d, GROUPS)
        return remote(
            psend.at[d, s], ret.at[grp], p_send.at[d, s], ret_recv.at[lax.rem(GROUPS - d, GROUPS)],
            at_z(gs * deep + s),
        ), o == direct

    def chain_copy(d, s, plus):
        zz = lax.rem(z - (plus * 2 - 1) + lines, lines)
        return remote(psend.at[d, s], rz.at[d, s], p_send.at[d, s], c_recv.at[d, s], at_z(zz))

    def side_copy(s, plus):
        zz = lax.rem(z - (plus * 2 - 1) + lines, lines)
        return remote(psend.at[0, s], side.at[1 - plus], p_send.at[0, s], side_recv.at[1 - plus], at_z(zz))

    def mine(d, s):
        at = pl.multiple_of(lax.rem(s, two) * gmax, gmax)
        return part[d, lax.div(s, two), pl.ds(at, gmax), :]

    def send_back(d, s, plus):
        _, more = onward(plus)

        @pl.when(more)
        def _():
            chain_copy(d, s, plus).wait_recv()
            psend[d, s] = (mine(d, s) + rz[d, s].astype(F32)).astype(BF16)

        @pl.when(jnp.logical_not(more))
        def _():
            psend[d, s] = mine(d, s).astype(BF16)

        own = d == 0
        home, last = home_copy(d, s, plus)
        near = s + plus * 2 - 1 == o
        to_home = jnp.logical_not(own) & last
        to_side = own & near
        pl.when(to_home)(home.start)
        pl.when(to_side)(side_copy(s, plus).start)
        pl.when(jnp.logical_not(to_home | to_side))(chain_copy(d, s, plus).start)

    def mirrored(kind, d, s):
        return kind, (GROUPS - d) % GROUPS, (deep if kind in (ARRIVE, BACK) else 2) - 1 - s

    def pick(values):
        if len(set(values)) == 1:
            return jnp.int32(values[0])
        return sum(i * v for i, v in zip(in_row, values))

    def way(d, s, r):
        return {3: 1, 1: 0, 2: int(s >= two), 0: int(s < r)}[d]

    for n, (kind, d0, s0, d1, s1) in enumerate(PLAN):
        if kind == WAIT_META:
            for j in range(1, lines):
                meta_copy(j).wait_recv()
            continue
        if kind == WAIT_W:
            for copy in w_copies:
                copy.wait()
            remote(
                wd_hbm.at[:, :, my_cols], wd.at[peer], wd_send.at[0], wd_recv.at[0], other_core
            ).wait_recv()
            continue
        if kind == SEND_OPP:
            opp.start()
            continue
        per_row = [(d0, s0), (d1, s1)]
        per_row += [mirrored(kind, *p)[1:] for p in per_row[::-1]]
        d, s = pick([p[0] for p in per_row]), pick([p[1] for p in per_row])
        if kind in (ARRIVE, BACK):
            plus = pick([way(*p, r) for r, p in enumerate(per_row)])
            (arrive if kind == ARRIVE else send_back)(d, s, plus)
        else:
            {SELECT: select, EXCHANGE: exchange, GATE_UP: gate_up, DOWN: down, COMBINE: combine}[kind](d, s)

    for t in range(1, GROUPS):
        gt = lax.rem(grp + t, GROUPS)
        remote(psend.at[t, o], ret.at[gt], p_send.at[t, o], ret_recv.at[t], at_z(z)).wait_recv()

    @pl.when(o < deep - 1)
    def _():
        side_copy(o, 1).wait_recv()

    @pl.when(o > 0)
    def _():
        side_copy(o, 0).wait_recv()

    own = mine(0, o)
    own = own + jnp.where(o < deep - 1, side[0].astype(F32), 0.0)
    own = own + jnp.where(o > 0, side[1].astype(F32), 0.0)
    ret[grp] = own.astype(BF16)
    mixed = mm_tn(place[...], ret[...].reshape(GROUPS * gmax, half))
    sq = jnp.zeros((tok, 128), F32)
    for i in range(half // 128):
        v = mixed[:, i * 128 : (i + 1) * 128]
        sq = sq + v * v
    sq_out[...] = sq
    q_copy = remote(sq_out, sq_in, q_send.at[0], q_recv.at[0], other_core)
    q_copy.start()
    q_copy.wait_recv()
    total = jnp.sum(sq_out[...] + sq_in[...], axis=1, keepdims=True)
    out_ref[...] = (mixed * lax.rsqrt(total / width + EPS) * out_gain[...]).astype(BF16)

    q_copy.wait_send()
    for j in range(1, lines):
        meta_copy(j).wait_send()
    opp.wait_send()
    nxt.wait_send()
    prv.wait_send()
    pl.when(o < deep - 1)(own_up.wait_send)
    pl.when(o > 0)(own_dn.wait_send)
    wd_copy.wait_send()

    def sent(d, s, plus):
        copy, more = z_copy(d, s, plus)
        pl.when(more)(copy.wait_send)
        chain_copy(d, s, plus).wait_send()

    for s in range(deep):
        sent(2, s, s // two)
        sent(3, s, 1)
        sent(1, s, 0)
    for j in range(1, deep):
        s = lax.rem(o + j, deep)
        sent(0, s, (s < o).astype(I32))
    for d in range(GROUPS):
        for h in range(2):
            h_copy(d, h).wait_send()
            d_copy(d, h).wait_send()
            for j in range(1, cols):
                x_to(*out_args, d, h, j).wait_send()
                x_to(*back_args, d, h, j).wait_send()


def body(tokens, in_gain, routing, gate_prob, w_gate, w_up, w_down, out_gain):
    ep_count = lax.axis_size("ep")
    loc, width, ff = w_gate.shape
    tok, top = routing.shape
    half = out_gain.shape[0]
    epg = loc * ep_count // GROUPS
    cap = max(2, tok * top // (2 * epg))
    gmax = epg * cap // top
    side = math.isqrt(ep_count // GROUPS)
    lines = ep_count // side
    cols, deep = side, side
    two = deep // 2
    pair = two * gmax
    piece = loc * two * cap
    m = cols * two * cap
    cfg = (lines, side, tok, top, cap, gmax, half, width, epg)
    vmem = pl.BlockSpec(memory_space=pltpu.VMEM)
    anyw = pl.BlockSpec(memory_space=pl.ANY)
    dma = pltpu.SemaphoreType.DMA
    scratch = [
        pltpu.VMEM(w_gate.shape, BF16),
        pltpu.VMEM(w_up.shape, BF16),
        pltpu.VMEM((2, loc, ff, half), BF16),
        pltpu.VMEM((GROUPS * gmax, tok), BF16),
        pltpu.VMEM((GROUPS, 2 * top, 2 * gmax), F32),
        pltpu.VMEM((GROUPS, deep, 2 * top, 2 * gmax), F32),
        pltpu.VMEM((GROUPS, gmax, half), BF16),
        pltpu.VMEM((GROUPS, 2, two, gmax, half), BF16),
        pltpu.VMEM((GROUPS, 2, pair, pair), BF16),
        pltpu.VMEM((GROUPS, 2, pair, pair), BF16),
        pltpu.VMEM((GROUPS, 2, cols, piece, half), BF16),
        pltpu.VMEM((2, GROUPS, 2, cols, piece, half), BF16),
        pltpu.VMEM((2, GROUPS, 2, loc, m, ff), BF16),
        pltpu.VMEM((GROUPS, 2, cols, piece, half), BF16),
        pltpu.VMEM((GROUPS, 2, cols, piece, half), BF16),
        pltpu.VMEM((GROUPS, 2, pair, half), F32),
        pltpu.VMEM((GROUPS, deep, gmax, half), BF16),
        pltpu.VMEM((GROUPS, deep, gmax, half), BF16),
        pltpu.VMEM((2, gmax, half), BF16),
        pltpu.VMEM((GROUPS, gmax, half), BF16),
        pltpu.VMEM((tok, 128), F32),
        pltpu.VMEM((tok, 128), F32),
        dma((3,)),
        dma((1,)),
        dma((1,)),
        dma((lines,)),
        dma((lines,)),
        dma((5,)),
        dma((GROUPS, deep)),
        dma((GROUPS, deep)),
        dma((GROUPS, 2, cols)),
        dma((GROUPS, 2, cols)),
        dma((GROUPS, 2)),
        dma((GROUPS, 2)),
        dma((GROUPS, 2)),
        dma((GROUPS, 2)),
        dma((GROUPS, 2, cols)),
        dma((GROUPS, 2, cols)),
        dma((GROUPS, deep)),
        dma((GROUPS, deep)),
        dma((2,)),
        dma((GROUPS,)),
        dma((1,)),
        dma((1,)),
    ]
    return pl.pallas_call(
        functools.partial(kernel, cfg),
        out_shape=jax.ShapeDtypeStruct((tok, half), BF16),
        in_specs=[vmem] * 5 + [anyw] * 3,
        out_specs=vmem,
        scratch_shapes=scratch,
        compiler_params=pltpu.CompilerParams(
            collective_id=0, has_side_effects=True, vmem_limit_bytes=60 * 1024 * 1024
        ),
    )(
        routing.T, gate_prob.T, tokens, in_gain.reshape(1, width), out_gain.reshape(1, half),
        w_gate, w_up, w_down,
    )


def solution(mesh):
    placed = (
        P(("grp", "ep"), None),
        P(),
        P(("grp", "ep"), None),
        P(("grp", "ep"), None),
        P("ep", None, "tp"),
        P("ep", None, "tp"),
        P("ep", "tp", None),
        P("tp"),
    )
    return jax.shard_map(
        body, mesh=mesh, in_specs=placed, out_specs=P(("grp", "ep"), "tp"), check_vma=False
    )
```

time: 193 us -> 161 us (0.83)
  Pallas kernels: 191 us -> 159 us
    pallas_call x1, Pallas kernels: 191 us -> 159 us  [body(): pl.pallas_call(functools.partial(kernel, cfg), out_shape=jax.ShapeDtypeSt...]
where the time goes in v2:
time: 161 us
  Pallas kernels  159 us (99%)
  local copies, waits for them, and re-layouts  1.67 us (1%)
    pallas_call x1, Pallas kernels, body(): pl.pallas_call(functools.partial(kernel, cfg), out_shape=jax.ShapeDtypeSt...  159 us

profile of v2, /device:TPU:33, one launch (start us, length us, event | category | flops | bytes accessed | tf_op | source)
XLA Modules:
  0.0 160.7 jit_solution(6874609654851208019)
XLA Ops:
  0.0 159.0 %shard_map.82 = bf16[128,1024]{1,0:T(8,128)(2,1)} custom-call(s32[4,128]{1,0:T(4,128)} %bitcast.6, f32[4,128]{1,0:T(4,128)} %bitcast.7, bf16[128,2048]{1,0:T(8,128)(2,1)} %tokens.1, f32[1,2048]{1,0:T(1,128)} %bitcast.4, f32[1,1024]{1,0:T(1,128)} %bitcast.5, bf16[2,2048,256]{2,1,0:T(8,128)(2,1)} %wg_hbm.1, bf16[2,2048,256]{2,1,0:T(8,128)(2,1)} %wu_hbm.1, ...), custom_call_target="tpu_custom_call" | custom-call | tf_op jit(solution)/shard_map/pallas_call | solution.py:474
  159.0 1.7 %copy.10 = bf16[128,1024]{1,0:T(8,128)(2,1)} copy(bf16[128,1024]{1,0:T(8,128)(2,1)} %shard_map.82) | data formatting | bytes 524288

commit v3 on v2

--- a/solution.py
+++ b/solution.py
@@ -28,42 +28,46 @@
     return lax.dot_general(a, b, (((0,), (0,)), ((), ())), preferred_element_type=F32)
 
 
-ARRIVE, BACK, SELECT, EXCHANGE, GATE_UP, DOWN, COMBINE, SEND_OPP, WAIT_META, WAIT_W = range(10)
+PARTS = 2
+ARRIVE, BACK, SELECT, EXCHANGE, GATE_UP, DOWN, COMBINE, SEND, WAIT_META, WAIT_W = range(10)
 
 PLAN = (
-    (ARRIVE, 0, 1, 0, 2), (ARRIVE, 3, 3, 0, 0), (WAIT_META, 0, 0, 0, 0), (SELECT, 0, 0, 0, 0),
-    (EXCHANGE, 0, 0, 0, 0), (WAIT_W, 0, 0, 0, 0), (GATE_UP, 0, 0, 0, 0), (DOWN, 0, 0, 0, 0),
-    (ARRIVE, 3, 2, 3, 3), (ARRIVE, 3, 1, 0, 3), (SELECT, 3, 1, 0, 1), (SEND_OPP, 0, 0, 0, 0),
-    (ARRIVE, 3, 0, 3, 2), (SELECT, 3, 0, 3, 1), (COMBINE, 0, 0, 0, 0), (EXCHANGE, 3, 1, 0, 1),
-    (GATE_UP, 3, 1, 0, 1), (DOWN, 3, 1, 0, 1), (ARRIVE, 0, 2, 3, 1), (ARRIVE, 0, 3, 1, 0),
-    (EXCHANGE, 3, 0, 3, 1), (GATE_UP, 3, 0, 3, 1), (DOWN, 3, 0, 3, 1), (ARRIVE, 2, 3, 1, 1),
-    (SELECT, 0, 1, 1, 0), (COMBINE, 3, 1, 0, 1), (ARRIVE, 1, 0, 3, 0), (ARRIVE, 2, 2, 1, 2),
-    (SELECT, 2, 1, 3, 0), (COMBINE, 3, 0, 3, 1), (ARRIVE, 1, 1, 1, 3), (ARRIVE, 1, 2, 2, 3),
-    (EXCHANGE, 0, 1, 1, 0), (SELECT, 1, 0, 1, 1), (ARRIVE, 1, 3, 2, 2), (SELECT, 1, 1, 2, 1),
-    (GATE_UP, 0, 1, 1, 0), (ARRIVE, 2, 0, 2, 0), (EXCHANGE, 2, 1, 3, 0), (DOWN, 0, 1, 1, 0),
-    (ARRIVE, 2, 1, 2, 1), (SELECT, 2, 0, 2, 0), (EXCHANGE, 1, 0, 1, 1), (GATE_UP, 1, 0, 3, 0),
-    (EXCHANGE, 1, 1, 2, 1), (GATE_UP, 2, 1, 1, 1), (DOWN, 2, 1, 3, 0), (BACK, 0, 1, 0, 2),
-    (DOWN, 1, 0, 1, 1), (GATE_UP, 1, 1, 2, 1), (COMBINE, 0, 1, 1, 0), (BACK, 0, 2, 0, 3),
-    (BACK, 0, 3, 0, 0), (DOWN, 1, 1, 2, 1), (EXCHANGE, 2, 0, 2, 0), (COMBINE, 1, 0, 1, 1),
-    (BACK, 1, 1, 1, 1), (GATE_UP, 2, 0, 2, 0), (BACK, 1, 0, 1, 0), (DOWN, 2, 0, 2, 0),
-    (COMBINE, 2, 1, 2, 1), (COMBINE, 1, 1, 3, 0), (BACK, 1, 3, 3, 2), (BACK, 1, 2, 1, 3),
-    (COMBINE, 2, 0, 2, 0), (BACK, 2, 0, 3, 3), (BACK, 2, 1, 1, 2), (BACK, 3, 2, 3, 0),
-    (BACK, 3, 3, 2, 0), (BACK, 3, 0, 3, 1), (BACK, 3, 1, 2, 1), (BACK, 2, 2, 2, 2),
-    (BACK, 2, 3, 2, 3),
+    (SEND, 0, 0, 0, 0), (SEND, 1, 0, 1, 0), (SEND, 3, 0, 3, 0), (ARRIVE, 0, 1, 0, 2),
+    (ARRIVE, 3, 3, 0, 0), (WAIT_META, 0, 0, 0, 0), (SELECT, 0, 0, 0, 0), (EXCHANGE, 0, 0, 0, 0),
+    (WAIT_W, 0, 0, 0, 0), (GATE_UP, 0, 0, 0, 0), (DOWN, 0, 0, 0, 0), (ARRIVE, 3, 2, 3, 3),
+    (ARRIVE, 3, 1, 0, 3), (SELECT, 3, 1, 0, 1), (SEND, 2, 0, 2, 0), (ARRIVE, 3, 0, 3, 2),
+    (SELECT, 3, 0, 3, 1), (COMBINE, 0, 0, 0, 0), (EXCHANGE, 3, 1, 0, 1), (GATE_UP, 3, 1, 0, 1),
+    (DOWN, 3, 1, 0, 1), (ARRIVE, 0, 2, 3, 1), (ARRIVE, 0, 3, 1, 0), (EXCHANGE, 3, 0, 3, 1),
+    (GATE_UP, 3, 0, 3, 1), (DOWN, 3, 0, 3, 1), (ARRIVE, 2, 3, 1, 1), (SELECT, 0, 1, 1, 0),
+    (COMBINE, 3, 1, 0, 1), (ARRIVE, 1, 0, 3, 0), (ARRIVE, 2, 2, 1, 2), (SELECT, 2, 1, 3, 0),
+    (COMBINE, 3, 0, 3, 1), (ARRIVE, 1, 1, 1, 3), (ARRIVE, 1, 2, 2, 3), (EXCHANGE, 0, 1, 1, 0),
+    (SELECT, 1, 0, 1, 1), (ARRIVE, 1, 3, 2, 2), (SELECT, 1, 1, 2, 1), (GATE_UP, 0, 1, 1, 0),
+    (ARRIVE, 2, 0, 2, 0), (EXCHANGE, 2, 1, 3, 0), (DOWN, 0, 1, 1, 0), (ARRIVE, 2, 1, 2, 1),
+    (SELECT, 2, 0, 2, 0), (EXCHANGE, 1, 0, 1, 1), (GATE_UP, 1, 0, 3, 0), (EXCHANGE, 1, 1, 2, 1),
+    (GATE_UP, 2, 1, 1, 1), (DOWN, 2, 1, 3, 0), (BACK, 0, 1, 0, 2), (DOWN, 1, 0, 1, 1),
+    (GATE_UP, 1, 1, 2, 1), (COMBINE, 0, 1, 1, 0), (BACK, 0, 2, 0, 3), (BACK, 0, 3, 0, 0),
+    (DOWN, 1, 1, 2, 1), (EXCHANGE, 2, 0, 2, 0), (COMBINE, 1, 0, 1, 1), (BACK, 1, 1, 1, 1),
+    (GATE_UP, 2, 0, 2, 0), (BACK, 1, 0, 1, 0), (DOWN, 2, 0, 2, 0), (COMBINE, 2, 1, 2, 1),
+    (COMBINE, 1, 1, 3, 0), (BACK, 1, 3, 3, 2), (BACK, 1, 2, 1, 3), (COMBINE, 2, 0, 2, 0),
+    (BACK, 2, 0, 3, 3), (BACK, 2, 1, 1, 2), (BACK, 3, 2, 3, 0), (BACK, 3, 3, 2, 0),
+    (BACK, 3, 0, 3, 1), (BACK, 3, 1, 2, 1), (BACK, 2, 2, 2, 2), (BACK, 2, 3, 2, 3),
 )
 
 
 def kernel(
     cfg, routing, prob, tokens, gain, out_gain, wg_hbm, wu_hbm, wd_hbm, out_ref,
     wg, wu, wd, place, meta_out, meta_in, packed, zbuf, mix_hi, mix_lo, xsend, rows, hid,
-    back_out, back_in, part, psend, rz, side, ret, sq_out, sq_in,
+    back_out, back_in, part, psend, land, ret, sq_out, sq_in,
     w_sem, wd_send, wd_recv, m_send, m_recv, i_send, z_send, z_recv, x_send, x_recv,
-    d_send, d_recv, h_send, h_recv, b_send, b_recv, p_send, c_recv, side_recv, ret_recv,
+    d_send, d_recv, h_send, h_recv, b_send, b_recv, p_send, l_recv,
     q_send, q_recv,
 ):
     lines, side_len, tok, top, cap, gmax, half, width, epg = cfg
     cols, deep = side_len, side_len
     two = deep // 2
+    bit = gmax // PARTS
+    bits = [pl.ds(q * bit, bit) for q in range(PARTS)]
+    home_at, side_at = GROUPS * deep, GROUPS * deep + GROUPS
     me = lax.axis_index("ep")
     core = lax.axis_index("tp")
     peer = 1 - core
@@ -151,25 +155,31 @@
     for j in range(1, lines):
         meta_copy(j).start()
 
-    def chunk(d, s):
-        return zbuf.at[d, lax.div(s, two), lax.rem(s, two)]
-
-    def first(t, row):
+    def chunk(d, s, q):
+        return zbuf.at[d, lax.div(s, two), lax.rem(s, two), bits[q]]
+
+    def first(t, row, i, d):
         gt = lax.rem(grp + t, GROUPS)
-        d = (GROUPS - t) % GROUPS
-        return remote(
-            packed.at[gt], chunk(d, o), i_send.at[t], z_recv.at[d, o], at_z(gt * deep + row)
-        )
-
-    opp = first(2, (deep - 1) * (1 - late))
-    nxt = first(1, 0)
-    prv = first(3, deep - 1)
-    own_up = remote(packed.at[grp], chunk(0, o), i_send.at[0], z_recv.at[0, o], at_z(lax.rem(z + 1, lines)))
-    own_dn = remote(packed.at[grp], chunk(0, o), i_send.at[4], z_recv.at[0, o], at_z(lax.rem(z + lines - 1, lines)))
-    pl.when(o < deep - 1)(own_up.start)
-    pl.when(o > 0)(own_dn.start)
-    nxt.start()
-    prv.start()
+        return [
+            remote(
+                packed.at[gt, bits[q]], chunk(d, o, q), i_send.at[i, q], z_recv.at[d, o, q], at_z(row(gt))
+            )
+            for q in range(PARTS)
+        ]
+
+    opp = first(2, lambda gt: gt * deep + (deep - 1) * (1 - late), 2, 2)
+    nxt = first(1, lambda gt: gt * deep, 1, 3)
+    prv = first(3, lambda gt: gt * deep + deep - 1, 3, 1)
+    own_up = first(0, lambda gt: lax.rem(z + 1, lines), 0, 0)
+    own_dn = first(0, lambda gt: lax.rem(z + lines - 1, lines), 4, 0)
+
+    def each(copies, what):
+        def run_all():
+            for copy in copies:
+                getattr(copy, what)()
+
+        return run_all
+
     wd_copy = remote(wd_hbm.at[:, :, peer_cols], wd.at[core], wd_send.at[0], wd_recv.at[0], other_core)
     wd_copy.start()
     zbuf[0, late, lax.rem(o, two)] = packed[grp]
@@ -180,14 +190,16 @@
         more = ((plus == 1) & (o < deep - 1)) | ((plus == 0) & (o > 0))
         return zz, more
 
-    def z_copy(d, s, plus):
+    def z_copy(d, s, plus, q):
         zz, more = onward(plus)
-        return remote(chunk(d, s), chunk(d, s), z_send.at[d, s], z_recv.at[d, s], at_z(zz)), more
+        here = chunk(d, s, q)
+        return remote(here, here, z_send.at[d, s, q], z_recv.at[d, s, q], at_z(zz)), more
 
     def arrive(d, s, plus):
-        copy, more = z_copy(d, s, plus)
-        copy.wait_recv()
-        pl.when(more)(copy.start)
+        for q in range(PARTS):
+            copy, more = z_copy(d, s, plus, q)
+            copy.wait_recv()
+            pl.when(more)(copy.start)
 
     pair = two * gmax
     run = two * cap
@@ -271,49 +283,39 @@
         res = back_in[d, h].reshape(pair, half)
         part[d, h] = mm_tn(mix_hi[d, h], res) + mm_tn(mix_lo[d, h], res)
 
-    def home_copy(d, s, plus):
-        direct = (deep - 1) * (1 - plus)
-        gs = lax.rem(grp + d, GROUPS)
+    def landing(d, s, q, at, zz):
         return remote(
-            psend.at[d, s], ret.at[grp], p_send.at[d, s], ret_recv.at[lax.rem(GROUPS - d, GROUPS)],
-            at_z(gs * deep + s),
-        ), o == direct
-
-    def chain_copy(d, s, plus):
-        zz = lax.rem(z - (plus * 2 - 1) + lines, lines)
-        return remote(psend.at[d, s], rz.at[d, s], p_send.at[d, s], c_recv.at[d, s], at_z(zz))
-
-    def side_copy(s, plus):
-        zz = lax.rem(z - (plus * 2 - 1) + lines, lines)
-        return remote(psend.at[0, s], side.at[1 - plus], p_send.at[0, s], side_recv.at[1 - plus], at_z(zz))
-
-    def mine(d, s):
-        at = pl.multiple_of(lax.rem(s, two) * gmax, gmax)
-        return part[d, lax.div(s, two), pl.ds(at, gmax), :]
+            psend.at[d, s, bits[q]], land.at[at, bits[q]], p_send.at[d, s, q], l_recv.at[at, q], at_z(zz)
+        )
+
+    def mine(d, s, q):
+        at = pl.multiple_of(lax.rem(s, two) * gmax + q * bit, bit)
+        return part[d, lax.div(s, two), pl.ds(at, bit), :]
 
     def send_back(d, s, plus):
         _, more = onward(plus)
-
-        @pl.when(more)
-        def _():
-            chain_copy(d, s, plus).wait_recv()
-            psend[d, s] = (mine(d, s) + rz[d, s].astype(F32)).astype(BF16)
-
-        @pl.when(jnp.logical_not(more))
-        def _():
-            psend[d, s] = mine(d, s).astype(BF16)
-
-        own = d == 0
-        home, last = home_copy(d, s, plus)
-        near = s + plus * 2 - 1 == o
-        to_home = jnp.logical_not(own) & last
-        to_side = own & near
-        pl.when(to_home)(home.start)
-        pl.when(to_side)(side_copy(s, plus).start)
-        pl.when(jnp.logical_not(to_home | to_side))(chain_copy(d, s, plus).start)
+        own = (d == 0).astype(I32)
+        home = (1 - own) * (o == (deep - 1) * (1 - plus)).astype(I32)
+        near = own * (s + plus * 2 - 1 == o).astype(I32)
+        chain = d * deep + s
+        at = home * (home_at + grp) + near * (side_at + 1 - plus) + (1 - home - near) * chain
+        beside = lax.rem(z - (plus * 2 - 1) + lines, lines)
+        zz = home * (lax.rem(grp + d, GROUPS) * deep + s) + (1 - home) * beside
+        for q in range(PARTS):
+
+            @pl.when(more)
+            def _():
+                landing(d, s, q, chain, z).wait_recv()
+                psend[d, s, bits[q]] = (mine(d, s, q) + land[chain, bits[q]].astype(F32)).astype(BF16)
+
+            @pl.when(jnp.logical_not(more))
+            def _():
+                psend[d, s, bits[q]] = mine(d, s, q).astype(BF16)
+
+            landing(d, s, q, at, zz).start()
 
     def mirrored(kind, d, s):
-        return kind, (GROUPS - d) % GROUPS, (deep if kind in (ARRIVE, BACK) else 2) - 1 - s
+        return (GROUPS - d) % GROUPS, (deep if kind in (ARRIVE, BACK) else 2) - 1 - s
 
     def pick(values):
         if len(set(values)) == 1:
@@ -335,11 +337,20 @@
                 wd_hbm.at[:, :, my_cols], wd.at[peer], wd_send.at[0], wd_recv.at[0], other_core
             ).wait_recv()
             continue
-        if kind == SEND_OPP:
-            opp.start()
+        per_row = [(d0, s0), (d1, s1)]
+        per_row += [mirrored(kind, *p) for p in per_row[::-1]]
+        if kind == SEND:
+            for t, copies in ((1, nxt), (2, opp), (3, prv)):
+                flags = [int(p[0] == t) for p in per_row]
+                if all(flags):
+                    each(copies, "start")()
+                elif any(flags):
+                    pl.when(pick(flags) == 1)(each(copies, "start"))
+            flags = [int(p[0] == 0) for p in per_row]
+            if any(flags):
+                pl.when((pick(flags) == 1) & (o < deep - 1))(each(own_up, "start"))
+                pl.when((pick(flags) == 1) & (o > 0))(each(own_dn, "start"))
             continue
-        per_row = [(d0, s0), (d1, s1)]
-        per_row += [mirrored(kind, *p)[1:] for p in per_row[::-1]]
         d, s = pick([p[0] for p in per_row]), pick([p[1] for p in per_row])
         if kind in (ARRIVE, BACK):
             plus = pick([way(*p, r) for r, p in enumerate(per_row)])
@@ -347,21 +358,25 @@
         else:
             {SELECT: select, EXCHANGE: exchange, GATE_UP: gate_up, DOWN: down, COMBINE: combine}[kind](d, s)
 
-    for t in range(1, GROUPS):
-        gt = lax.rem(grp + t, GROUPS)
-        remote(psend.at[t, o], ret.at[gt], p_send.at[t, o], ret_recv.at[t], at_z(z)).wait_recv()
+    own = jnp.concatenate([mine(0, o, q) for q in range(PARTS)], axis=0)
 
     @pl.when(o < deep - 1)
     def _():
-        side_copy(o, 1).wait_recv()
+        for q in range(PARTS):
+            landing(0, o, q, side_at, z).wait_recv()
 
     @pl.when(o > 0)
     def _():
-        side_copy(o, 0).wait_recv()
-
-    own = mine(0, o)
-    own = own + jnp.where(o < deep - 1, side[0].astype(F32), 0.0)
-    own = own + jnp.where(o > 0, side[1].astype(F32), 0.0)
+        for q in range(PARTS):
+            landing(0, o, q, side_at + 1, z).wait_recv()
+
+    own = own + jnp.where(o < deep - 1, land[side_at].astype(F32), 0.0)
+    own = own + jnp.where(o > 0, land[side_at + 1].astype(F32), 0.0)
+    for t in (1, 3, 2):
+        gt = lax.rem(grp + t, GROUPS)
+        for q in range(PARTS):
+            landing(0, o, q, home_at + gt, z).wait_recv()
+    ret[...] = land[home_at : home_at + GROUPS]
     ret[grp] = own.astype(BF16)
     mixed = mm_tn(place[...], ret[...].reshape(GROUPS * gmax, half))
     sq = jnp.zeros((tok, 128), F32)
@@ -378,17 +393,16 @@
     q_copy.wait_send()
     for j in range(1, lines):
         meta_copy(j).wait_send()
-    opp.wait_send()
-    nxt.wait_send()
-    prv.wait_send()
-    pl.when(o < deep - 1)(own_up.wait_send)
-    pl.when(o > 0)(own_dn.wait_send)
+    each(opp + nxt + prv, "wait_send")()
+    pl.when(o < deep - 1)(each(own_up, "wait_send"))
+    pl.when(o > 0)(each(own_dn, "wait_send"))
     wd_copy.wait_send()
 
     def sent(d, s, plus):
-        copy, more = z_copy(d, s, plus)
-        pl.when(more)(copy.wait_send)
-        chain_copy(d, s, plus).wait_send()
+        copies, more = [z_copy(d, s, plus, q)[0] for q in range(PARTS)], onward(plus)[1]
+        pl.when(more)(each(copies, "wait_send"))
+        for q in range(PARTS):
+            landing(d, s, q, 0, z).wait_send()
 
     for s in range(deep):
         sent(2, s, s // two)
@@ -443,8 +457,7 @@
         pltpu.VMEM((GROUPS, 2, cols, piece, half), BF16),
         pltpu.VMEM((GROUPS, 2, pair, half), F32),
         pltpu.VMEM((GROUPS, deep, gmax, half), BF16),
-        pltpu.VMEM((GROUPS, deep, gmax, half), BF16),
-        pltpu.VMEM((2, gmax, half), BF16),
+        pltpu.VMEM((GROUPS * deep + GROUPS + 2, gmax, half), BF16),
         pltpu.VMEM((GROUPS, gmax, half), BF16),
         pltpu.VMEM((tok, 128), F32),
         pltpu.VMEM((tok, 128), F32),
@@ -453,9 +466,9 @@
         dma((1,)),
         dma((lines,)),
         dma((lines,)),
-        dma((5,)),
-        dma((GROUPS, deep)),
-        dma((GROUPS, deep)),
+        dma((5, PARTS)),
+        dma((GROUPS, deep, PARTS)),
+        dma((GROUPS, deep, PARTS)),
         dma((GROUPS, 2, cols)),
         dma((GROUPS, 2, cols)),
         dma((GROUPS, 2)),
@@ -464,10 +477,8 @@
         dma((GROUPS, 2)),
         dma((GROUPS, 2, cols)),
         dma((GROUPS, 2, cols)),
-        dma((GROUPS, deep)),
-        dma((GROUPS, deep)),
-        dma((2,)),
-        dma((GROUPS,)),
+        dma((GROUPS, deep, PARTS)),
+        dma((GROUPS * deep + GROUPS + 2, PARTS)),
         dma((1,)),
         dma((1,)),
     ]

time: 161 us -> 158 us (0.981)
  Pallas kernels: 159 us -> 156 us
    pallas_call x1, Pallas kernels: 159 us -> 156 us  [body(): pl.pallas_call(functools.partial(kernel, cfg), out_shape=jax.ShapeDtypeSt...]
where the time goes in v3:
time: 158 us
  Pallas kernels  156 us (99%)
  local copies, waits for them, and re-layouts  1.67 us (1%)
    pallas_call x1, Pallas kernels, body(): pl.pallas_call(functools.partial(kernel, cfg), out_shape=jax.ShapeDtypeSt...  156 us

profile of v3, /device:TPU:33, one launch (start us, length us, event | category | flops | bytes accessed | tf_op | source)
XLA Modules:
  0.0 158.0 jit_solution(8091896494185335030)
XLA Ops:
  0.0 156.3 %shard_map.82 = bf16[128,1024]{1,0:T(8,128)(2,1)} custom-call(s32[4,128]{1,0:T(4,128)} %bitcast.6, f32[4,128]{1,0:T(4,128)} %bitcast.7, bf16[128,2048]{1,0:T(8,128)(2,1)} %tokens.1, f32[1,2048]{1,0:T(1,128)} %bitcast.4, f32[1,1024]{1,0:T(1,128)} %bitcast.5, bf16[2,2048,256]{2,1,0:T(8,128)(2,1)} %wg_hbm.1, bf16[2,2048,256]{2,1,0:T(8,128)(2,1)} %wu_hbm.1, ...), custom_call_target="tpu_custom_call" | custom-call | tf_op jit(solution)/shard_map/pallas_call | solution.py:485
  156.3 1.7 %copy.10 = bf16[128,1024]{1,0:T(8,128)(2,1)} copy(bf16[128,1024]{1,0:T(8,128)(2,1)} %shard_map.82) | data formatting | bytes 524288

commit v4 on v3

--- a/solution.py
+++ b/solution.py
@@ -32,25 +32,25 @@
 ARRIVE, BACK, SELECT, EXCHANGE, GATE_UP, DOWN, COMBINE, SEND, WAIT_META, WAIT_W = range(10)
 
 PLAN = (
-    (SEND, 0, 0, 0, 0), (SEND, 1, 0, 1, 0), (SEND, 3, 0, 3, 0), (ARRIVE, 0, 1, 0, 2),
-    (ARRIVE, 3, 3, 0, 0), (WAIT_META, 0, 0, 0, 0), (SELECT, 0, 0, 0, 0), (EXCHANGE, 0, 0, 0, 0),
-    (WAIT_W, 0, 0, 0, 0), (GATE_UP, 0, 0, 0, 0), (DOWN, 0, 0, 0, 0), (ARRIVE, 3, 2, 3, 3),
-    (ARRIVE, 3, 1, 0, 3), (SELECT, 3, 1, 0, 1), (SEND, 2, 0, 2, 0), (ARRIVE, 3, 0, 3, 2),
-    (SELECT, 3, 0, 3, 1), (COMBINE, 0, 0, 0, 0), (EXCHANGE, 3, 1, 0, 1), (GATE_UP, 3, 1, 0, 1),
-    (DOWN, 3, 1, 0, 1), (ARRIVE, 0, 2, 3, 1), (ARRIVE, 0, 3, 1, 0), (EXCHANGE, 3, 0, 3, 1),
-    (GATE_UP, 3, 0, 3, 1), (DOWN, 3, 0, 3, 1), (ARRIVE, 2, 3, 1, 1), (SELECT, 0, 1, 1, 0),
-    (COMBINE, 3, 1, 0, 1), (ARRIVE, 1, 0, 3, 0), (ARRIVE, 2, 2, 1, 2), (SELECT, 2, 1, 3, 0),
-    (COMBINE, 3, 0, 3, 1), (ARRIVE, 1, 1, 1, 3), (ARRIVE, 1, 2, 2, 3), (EXCHANGE, 0, 1, 1, 0),
-    (SELECT, 1, 0, 1, 1), (ARRIVE, 1, 3, 2, 2), (SELECT, 1, 1, 2, 1), (GATE_UP, 0, 1, 1, 0),
-    (ARRIVE, 2, 0, 2, 0), (EXCHANGE, 2, 1, 3, 0), (DOWN, 0, 1, 1, 0), (ARRIVE, 2, 1, 2, 1),
-    (SELECT, 2, 0, 2, 0), (EXCHANGE, 1, 0, 1, 1), (GATE_UP, 1, 0, 3, 0), (EXCHANGE, 1, 1, 2, 1),
-    (GATE_UP, 2, 1, 1, 1), (DOWN, 2, 1, 3, 0), (BACK, 0, 1, 0, 2), (DOWN, 1, 0, 1, 1),
-    (GATE_UP, 1, 1, 2, 1), (COMBINE, 0, 1, 1, 0), (BACK, 0, 2, 0, 3), (BACK, 0, 3, 0, 0),
-    (DOWN, 1, 1, 2, 1), (EXCHANGE, 2, 0, 2, 0), (COMBINE, 1, 0, 1, 1), (BACK, 1, 1, 1, 1),
-    (GATE_UP, 2, 0, 2, 0), (BACK, 1, 0, 1, 0), (DOWN, 2, 0, 2, 0), (COMBINE, 2, 1, 2, 1),
-    (COMBINE, 1, 1, 3, 0), (BACK, 1, 3, 3, 2), (BACK, 1, 2, 1, 3), (COMBINE, 2, 0, 2, 0),
-    (BACK, 2, 0, 3, 3), (BACK, 2, 1, 1, 2), (BACK, 3, 2, 3, 0), (BACK, 3, 3, 2, 0),
-    (BACK, 3, 0, 3, 1), (BACK, 3, 1, 2, 1), (BACK, 2, 2, 2, 2), (BACK, 2, 3, 2, 3),
+    (SEND, 0, 0, 0, 0), (SEND, 3, 0, 3, 0), (ARRIVE, 3, 3, 0, 0), (ARRIVE, 3, 2, 0, 2),
+    (ARRIVE, 0, 1, 0, 3), (SEND, 2, 0, 1, 0), (WAIT_META, 0, 0, 0, 0), (SELECT, 0, 0, 0, 0),
+    (EXCHANGE, 0, 0, 0, 0), (SEND, 1, 0, 2, 0), (WAIT_W, 0, 0, 0, 0), (GATE_UP, 0, 0, 0, 0),
+    (SELECT, 3, 1, 0, 1), (DOWN, 0, 0, 0, 0), (ARRIVE, 3, 0, 3, 3), (EXCHANGE, 3, 1, 0, 1),
+    (ARRIVE, 0, 2, 3, 2), (ARRIVE, 3, 1, 1, 0), (ARRIVE, 0, 3, 3, 0), (ARRIVE, 2, 3, 1, 1),
+    (SELECT, 3, 0, 3, 1), (SELECT, 0, 1, 1, 0), (ARRIVE, 2, 2, 3, 1), (SELECT, 2, 1, 3, 0),
+    (ARRIVE, 1, 0, 1, 3), (ARRIVE, 1, 3, 2, 3), (ARRIVE, 1, 1, 1, 2), (GATE_UP, 3, 1, 0, 1),
+    (DOWN, 3, 1, 0, 1), (ARRIVE, 2, 0, 2, 2), (SELECT, 1, 0, 2, 1), (ARRIVE, 1, 2, 2, 0),
+    (EXCHANGE, 0, 1, 1, 0), (ARRIVE, 2, 1, 2, 1), (SELECT, 1, 1, 1, 1), (EXCHANGE, 2, 1, 3, 0),
+    (GATE_UP, 0, 1, 1, 0), (EXCHANGE, 1, 0, 3, 1), (DOWN, 0, 1, 1, 0), (GATE_UP, 1, 0, 3, 0),
+    (EXCHANGE, 1, 1, 1, 1), (COMBINE, 0, 0, 1, 0), (EXCHANGE, 3, 0, 2, 1), (SELECT, 2, 0, 2, 0),
+    (GATE_UP, 2, 1, 1, 1), (GATE_UP, 1, 1, 3, 1), (DOWN, 1, 0, 1, 1), (COMBINE, 0, 1, 0, 1),
+    (BACK, 0, 3, 0, 3), (EXCHANGE, 2, 0, 2, 0), (DOWN, 1, 1, 3, 1), (BACK, 0, 2, 1, 0),
+    (GATE_UP, 3, 0, 2, 0), (COMBINE, 1, 0, 0, 0), (DOWN, 2, 1, 2, 0), (BACK, 1, 0, 1, 1),
+    (GATE_UP, 2, 0, 2, 1), (BACK, 1, 1, 0, 2), (DOWN, 2, 0, 2, 1), (COMBINE, 1, 1, 3, 1),
+    (BACK, 1, 2, 3, 3), (COMBINE, 2, 0, 2, 0), (DOWN, 3, 0, 3, 0), (BACK, 2, 0, 3, 2),
+    (COMBINE, 3, 1, 2, 1), (BACK, 2, 1, 2, 0), (BACK, 1, 3, 0, 0), (COMBINE, 3, 0, 1, 1),
+    (BACK, 3, 3, 2, 1), (BACK, 3, 2, 1, 2), (BACK, 0, 1, 2, 3), (COMBINE, 2, 1, 3, 0),
+    (BACK, 2, 3, 2, 2), (BACK, 2, 2, 1, 3), (BACK, 3, 1, 3, 1), (BACK, 3, 0, 3, 0),
 )
 
 

time: 158 us -> 144 us (0.911)
  Pallas kernels: 156 us -> 142 us
    pallas_call x1, Pallas kernels: 156 us -> 142 us  [body(): pl.pallas_call(functools.partial(kernel, cfg), out_shape=jax.ShapeDtypeSt...]
where the time goes in v4:
time: 144 us
  Pallas kernels  142 us (99%)
  local copies, waits for them, and re-layouts  1.67 us (1%)
    pallas_call x1, Pallas kernels, body(): pl.pallas_call(functools.partial(kernel, cfg), out_shape=jax.ShapeDtypeSt...  142 us

profile of v4, /device:TPU:33, one launch (start us, length us, event | category | flops | bytes accessed | tf_op | source)
XLA Modules:
  0.0 143.7 jit_solution(12890873779468596845)
XLA Ops:
  0.0 142.0 %shard_map.82 = bf16[128,1024]{1,0:T(8,128)(2,1)} custom-call(s32[4,128]{1,0:T(4,128)} %bitcast.6, f32[4,128]{1,0:T(4,128)} %bitcast.7, bf16[128,2048]{1,0:T(8,128)(2,1)} %tokens.1, f32[1,2048]{1,0:T(1,128)} %bitcast.4, f32[1,1024]{1,0:T(1,128)} %bitcast.5, bf16[2,2048,256]{2,1,0:T(8,128)(2,1)} %wg_hbm.1, bf16[2,2048,256]{2,1,0:T(8,128)(2,1)} %wu_hbm.1, ...), custom_call_target="tpu_custom_call" | custom-call | tf_op jit(solution)/shard_map/pallas_call | solution.py:485
  142.0 1.7 %copy.10 = bf16[128,1024]{1,0:T(8,128)(2,1)} copy(bf16[128,1024]{1,0:T(8,128)(2,1)} %shard_map.82) | data formatting | bytes 524288

commit v5 on v4

--- a/solution.py
+++ b/solution.py
@@ -29,35 +29,35 @@
 
 
 PARTS = 2
-ARRIVE, BACK, SELECT, EXCHANGE, GATE_UP, DOWN, COMBINE, SEND, WAIT_META, WAIT_W = range(10)
+ARRIVE, BACK, SELECT, EXCHANGE, GATE_UP, DOWN, COMBINE, SEND, METAS, WAIT_W = range(10)
 
 PLAN = (
-    (SEND, 0, 0, 0, 0), (SEND, 3, 0, 3, 0), (ARRIVE, 3, 3, 0, 0), (ARRIVE, 3, 2, 0, 2),
-    (ARRIVE, 0, 1, 0, 3), (SEND, 2, 0, 1, 0), (WAIT_META, 0, 0, 0, 0), (SELECT, 0, 0, 0, 0),
-    (EXCHANGE, 0, 0, 0, 0), (SEND, 1, 0, 2, 0), (WAIT_W, 0, 0, 0, 0), (GATE_UP, 0, 0, 0, 0),
-    (SELECT, 3, 1, 0, 1), (DOWN, 0, 0, 0, 0), (ARRIVE, 3, 0, 3, 3), (EXCHANGE, 3, 1, 0, 1),
-    (ARRIVE, 0, 2, 3, 2), (ARRIVE, 3, 1, 1, 0), (ARRIVE, 0, 3, 3, 0), (ARRIVE, 2, 3, 1, 1),
-    (SELECT, 3, 0, 3, 1), (SELECT, 0, 1, 1, 0), (ARRIVE, 2, 2, 3, 1), (SELECT, 2, 1, 3, 0),
-    (ARRIVE, 1, 0, 1, 3), (ARRIVE, 1, 3, 2, 3), (ARRIVE, 1, 1, 1, 2), (GATE_UP, 3, 1, 0, 1),
-    (DOWN, 3, 1, 0, 1), (ARRIVE, 2, 0, 2, 2), (SELECT, 1, 0, 2, 1), (ARRIVE, 1, 2, 2, 0),
-    (EXCHANGE, 0, 1, 1, 0), (ARRIVE, 2, 1, 2, 1), (SELECT, 1, 1, 1, 1), (EXCHANGE, 2, 1, 3, 0),
-    (GATE_UP, 0, 1, 1, 0), (EXCHANGE, 1, 0, 3, 1), (DOWN, 0, 1, 1, 0), (GATE_UP, 1, 0, 3, 0),
-    (EXCHANGE, 1, 1, 1, 1), (COMBINE, 0, 0, 1, 0), (EXCHANGE, 3, 0, 2, 1), (SELECT, 2, 0, 2, 0),
-    (GATE_UP, 2, 1, 1, 1), (GATE_UP, 1, 1, 3, 1), (DOWN, 1, 0, 1, 1), (COMBINE, 0, 1, 0, 1),
-    (BACK, 0, 3, 0, 3), (EXCHANGE, 2, 0, 2, 0), (DOWN, 1, 1, 3, 1), (BACK, 0, 2, 1, 0),
-    (GATE_UP, 3, 0, 2, 0), (COMBINE, 1, 0, 0, 0), (DOWN, 2, 1, 2, 0), (BACK, 1, 0, 1, 1),
-    (GATE_UP, 2, 0, 2, 1), (BACK, 1, 1, 0, 2), (DOWN, 2, 0, 2, 1), (COMBINE, 1, 1, 3, 1),
-    (BACK, 1, 2, 3, 3), (COMBINE, 2, 0, 2, 0), (DOWN, 3, 0, 3, 0), (BACK, 2, 0, 3, 2),
-    (COMBINE, 3, 1, 2, 1), (BACK, 2, 1, 2, 0), (BACK, 1, 3, 0, 0), (COMBINE, 3, 0, 1, 1),
-    (BACK, 3, 3, 2, 1), (BACK, 3, 2, 1, 2), (BACK, 0, 1, 2, 3), (COMBINE, 2, 1, 3, 0),
-    (BACK, 2, 3, 2, 2), (BACK, 2, 2, 1, 3), (BACK, 3, 1, 3, 1), (BACK, 3, 0, 3, 0),
+    (SEND, 1, 0, 0, 0), (SEND, 0, 0, 3, 0), (SEND, 3, 0, 1, 0), (METAS, 0, 0, 0, 0),
+    (ARRIVE, 3, 0, 0, 2), (ARRIVE, 0, 1, 0, 0), (SELECT, 0, 0, 0, 0), (ARRIVE, 3, 2, 3, 2),
+    (ARRIVE, 0, 2, 3, 0), (ARRIVE, 3, 3, 0, 3), (SELECT, 3, 1, 0, 1), (SEND, 2, 0, 2, 0),
+    (EXCHANGE, 0, 0, 0, 0), (WAIT_W, 0, 0, 0, 0), (GATE_UP, 0, 0, 0, 0), (ARRIVE, 0, 3, 3, 3),
+    (SELECT, 0, 1, 3, 1), (DOWN, 0, 0, 0, 0), (ARRIVE, 3, 1, 1, 1), (ARRIVE, 2, 3, 3, 1),
+    (ARRIVE, 2, 2, 1, 0), (EXCHANGE, 3, 1, 3, 1), (SELECT, 3, 0, 1, 0), (GATE_UP, 3, 1, 3, 1),
+    (ARRIVE, 1, 1, 1, 3), (ARRIVE, 1, 0, 2, 3), (SELECT, 1, 0, 3, 0), (ARRIVE, 1, 3, 2, 2),
+    (EXCHANGE, 0, 1, 1, 0), (EXCHANGE, 3, 0, 0, 1), (SELECT, 2, 1, 2, 1), (ARRIVE, 1, 2, 1, 2),
+    (GATE_UP, 3, 0, 1, 0), (SELECT, 1, 1, 1, 1), (GATE_UP, 0, 1, 0, 1), (DOWN, 0, 1, 1, 0),
+    (ARRIVE, 2, 0, 2, 1), (DOWN, 3, 1, 0, 1), (EXCHANGE, 1, 0, 2, 1), (ARRIVE, 2, 1, 2, 0),
+    (COMBINE, 0, 1, 0, 1), (COMBINE, 0, 0, 1, 0), (EXCHANGE, 1, 1, 3, 0), (SELECT, 2, 0, 2, 0),
+    (BACK, 0, 2, 0, 2), (EXCHANGE, 2, 1, 1, 1), (GATE_UP, 1, 0, 2, 1), (DOWN, 1, 0, 3, 1),
+    (BACK, 0, 3, 0, 3), (GATE_UP, 1, 1, 1, 1), (EXCHANGE, 2, 0, 2, 0), (DOWN, 1, 1, 2, 1),
+    (GATE_UP, 2, 0, 2, 0), (COMBINE, 1, 0, 3, 1), (DOWN, 2, 0, 2, 0), (BACK, 1, 0, 1, 0),
+    (COMBINE, 3, 1, 0, 0), (GATE_UP, 2, 1, 3, 0), (BACK, 1, 1, 1, 1), (COMBINE, 2, 0, 2, 1),
+    (BACK, 2, 1, 3, 3), (DOWN, 3, 0, 1, 1), (DOWN, 2, 1, 3, 0), (BACK, 2, 0, 0, 0),
+    (COMBINE, 1, 1, 2, 0), (BACK, 1, 2, 2, 1), (BACK, 3, 3, 2, 0), (BACK, 1, 3, 2, 2),
+    (COMBINE, 2, 1, 1, 1), (BACK, 2, 2, 3, 2), (BACK, 3, 2, 2, 3), (BACK, 2, 3, 1, 2),
+    (BACK, 0, 1, 1, 3), (COMBINE, 3, 0, 3, 0), (BACK, 3, 1, 3, 1), (BACK, 3, 0, 3, 0),
 )
 
 
 def kernel(
     cfg, routing, prob, tokens, gain, out_gain, wg_hbm, wu_hbm, wd_hbm, out_ref,
     wg, wu, wd, place, meta_out, meta_in, packed, zbuf, mix_hi, mix_lo, xsend, rows, hid,
-    back_out, back_in, part, psend, land, ret, sq_out, sq_in,
+    back_out, back_in, part, psend, land, sq_out, sq_in,
     w_sem, wd_send, wd_recv, m_send, m_recv, i_send, z_send, z_recv, x_send, x_recv,
     d_send, d_recv, h_send, h_recv, b_send, b_recv, p_send, l_recv,
     q_send, q_recv,
@@ -145,15 +145,27 @@
     def rel(a):
         return lax.rem(a + 2 * GROUPS, GROUPS)
 
-    def meta_copy(j):
-        zt = lax.rem(z + j, lines)
-        gt = lax.div(zt, deep)
+    def meta_near(j):
+        s = lax.rem(o + j, deep)
         return remote(
-            meta_out.at[gt], meta_in.at[rel(grp - gt), o], m_send.at[j], m_recv.at[j], at_z(zt)
+            meta_out.at[grp], meta_in.at[0, o], m_send.at[j], m_recv.at[0, o], at_z(grp * deep + s)
         )
 
-    for j in range(1, lines):
-        meta_copy(j).start()
+    def meta_group(t):
+        gt = lax.rem(grp + t, GROUPS)
+        d = GROUPS - t
+        return [
+            remote(
+                meta_out.at[gt], meta_in.at[d, o], m_send.at[t * deep + s], m_recv.at[d, o],
+                at_z(gt * deep + s),
+            )
+            for s in range(deep)
+        ]
+
+    near_metas = [meta_near(j) for j in range(1, deep)]
+    far_metas = [copy for t in (1, 3, 2) for copy in meta_group(t)]
+    for copy in near_metas:
+        copy.start()
 
     def chunk(d, s, q):
         return zbuf.at[d, lax.div(s, two), lax.rem(s, two), bits[q]]
@@ -223,6 +235,11 @@
         return remote(rows.at[peer, d, h], rows.at[peer, d, h], d_send.at[d, h], d_recv.at[d, h], other_core)
 
     def select(d, h):
+        for i in range(two):
+            s = two * h + i
+            pl.when((d != 0) | (s != o))(
+                remote(meta_out.at[0], meta_in.at[d, s], m_send.at[0], m_recv.at[d, s], at_z(z)).wait_recv
+            )
         lane = iota((2 * top, 2 * gmax), 1)
         info = jnp.where(lane < gmax, meta_in[d, two * h], meta_in[d, two * h + 1])
         zs = lax.div(iota((1, pair), 1), gmax)
@@ -326,9 +343,8 @@
         return {3: 1, 1: 0, 2: int(s >= two), 0: int(s < r)}[d]
 
     for n, (kind, d0, s0, d1, s1) in enumerate(PLAN):
-        if kind == WAIT_META:
-            for j in range(1, lines):
-                meta_copy(j).wait_recv()
+        if kind == METAS:
+            each(far_metas, "start")()
             continue
         if kind == WAIT_W:
             for copy in w_copies:
@@ -376,9 +392,9 @@
         gt = lax.rem(grp + t, GROUPS)
         for q in range(PARTS):
             landing(0, o, q, home_at + gt, z).wait_recv()
-    ret[...] = land[home_at : home_at + GROUPS]
-    ret[grp] = own.astype(BF16)
-    mixed = mm_tn(place[...], ret[...].reshape(GROUPS * gmax, half))
+    land[home_at + grp] = own.astype(BF16)
+    returned = land[home_at : home_at + GROUPS].reshape(GROUPS * gmax, half)
+    mixed = mm_tn(place[...], returned)
     sq = jnp.zeros((tok, 128), F32)
     for i in range(half // 128):
         v = mixed[:, i * 128 : (i + 1) * 128]
@@ -391,8 +407,7 @@
     out_ref[...] = (mixed * lax.rsqrt(total / width + EPS) * out_gain[...]).astype(BF16)
 
     q_copy.wait_send()
-    for j in range(1, lines):
-        meta_copy(j).wait_send()
+    each(near_metas + far_metas, "wait_send")()
     each(opp + nxt + prv, "wait_send")()
     pl.when(o < deep - 1)(each(own_up, "wait_send"))
     pl.when(o > 0)(each(own_dn, "wait_send"))
@@ -458,14 +473,13 @@
         pltpu.VMEM((GROUPS, 2, pair, half), F32),
         pltpu.VMEM((GROUPS, deep, gmax, half), BF16),
         pltpu.VMEM((GROUPS * deep + GROUPS + 2, gmax, half), BF16),
-        pltpu.VMEM((GROUPS, gmax, half), BF16),
         pltpu.VMEM((tok, 128), F32),
         pltpu.VMEM((tok, 128), F32),
         dma((3,)),
         dma((1,)),
         dma((1,)),
         dma((lines,)),
-        dma((lines,)),
+        dma((GROUPS, deep)),
         dma((5, PARTS)),
         dma((GROUPS, deep, PARTS)),
         dma((GROUPS, deep, PARTS)),

time: 144 us -> 139 us (0.965)
  Pallas kernels: 142 us -> 137 us
    pallas_call x1, Pallas kernels: 142 us -> 137 us  [body(): pl.pallas_call(functools.partial(kernel, cfg), out_shape=jax.ShapeDtypeSt...]
where the time goes in v5:
time: 139 us
  Pallas kernels  137 us (99%)
  local copies, waits for them, and re-layouts  1.67 us (1%)
    pallas_call x1, Pallas kernels, body(): pl.pallas_call(functools.partial(kernel, cfg), out_shape=jax.ShapeDtypeSt...  137 us

profile of v5, /device:TPU:33, one launch (start us, length us, event | category | flops | bytes accessed | tf_op | source)
XLA Modules:
  0.0 139.1 jit_solution(10724044250867079306)
XLA Ops:
  0.0 137.4 %shard_map.82 = bf16[128,1024]{1,0:T(8,128)(2,1)} custom-call(s32[4,128]{1,0:T(4,128)} %bitcast.6, f32[4,128]{1,0:T(4,128)} %bitcast.7, bf16[128,2048]{1,0:T(8,128)(2,1)} %tokens.1, f32[1,2048]{1,0:T(1,128)} %bitcast.4, f32[1,1024]{1,0:T(1,128)} %bitcast.5, bf16[2,2048,256]{2,1,0:T(8,128)(2,1)} %wg_hbm.1, bf16[2,2048,256]{2,1,0:T(8,128)(2,1)} %wu_hbm.1, ...), custom_call_target="tpu_custom_call" | custom-call | tf_op jit(solution)/shard_map/pallas_call | solution.py:499
  137.4 1.7 %copy.10 = bf16[128,1024]{1,0:T(8,128)(2,1)} copy(bf16[128,1024]{1,0:T(8,128)(2,1)} %shard_map.82) | data formatting | bytes 524288

commit v6 on v5

--- a/solution.py
+++ b/solution.py
@@ -28,29 +28,29 @@
     return lax.dot_general(a, b, (((0,), (0,)), ((), ())), preferred_element_type=F32)
 
 
-PARTS = 2
+PARTS = 4
 ARRIVE, BACK, SELECT, EXCHANGE, GATE_UP, DOWN, COMBINE, SEND, METAS, WAIT_W = range(10)
 
 PLAN = (
-    (SEND, 1, 0, 0, 0), (SEND, 0, 0, 3, 0), (SEND, 3, 0, 1, 0), (METAS, 0, 0, 0, 0),
-    (ARRIVE, 3, 0, 0, 2), (ARRIVE, 0, 1, 0, 0), (SELECT, 0, 0, 0, 0), (ARRIVE, 3, 2, 3, 2),
-    (ARRIVE, 0, 2, 3, 0), (ARRIVE, 3, 3, 0, 3), (SELECT, 3, 1, 0, 1), (SEND, 2, 0, 2, 0),
-    (EXCHANGE, 0, 0, 0, 0), (WAIT_W, 0, 0, 0, 0), (GATE_UP, 0, 0, 0, 0), (ARRIVE, 0, 3, 3, 3),
-    (SELECT, 0, 1, 3, 1), (DOWN, 0, 0, 0, 0), (ARRIVE, 3, 1, 1, 1), (ARRIVE, 2, 3, 3, 1),
-    (ARRIVE, 2, 2, 1, 0), (EXCHANGE, 3, 1, 3, 1), (SELECT, 3, 0, 1, 0), (GATE_UP, 3, 1, 3, 1),
-    (ARRIVE, 1, 1, 1, 3), (ARRIVE, 1, 0, 2, 3), (SELECT, 1, 0, 3, 0), (ARRIVE, 1, 3, 2, 2),
-    (EXCHANGE, 0, 1, 1, 0), (EXCHANGE, 3, 0, 0, 1), (SELECT, 2, 1, 2, 1), (ARRIVE, 1, 2, 1, 2),
-    (GATE_UP, 3, 0, 1, 0), (SELECT, 1, 1, 1, 1), (GATE_UP, 0, 1, 0, 1), (DOWN, 0, 1, 1, 0),
-    (ARRIVE, 2, 0, 2, 1), (DOWN, 3, 1, 0, 1), (EXCHANGE, 1, 0, 2, 1), (ARRIVE, 2, 1, 2, 0),
-    (COMBINE, 0, 1, 0, 1), (COMBINE, 0, 0, 1, 0), (EXCHANGE, 1, 1, 3, 0), (SELECT, 2, 0, 2, 0),
-    (BACK, 0, 2, 0, 2), (EXCHANGE, 2, 1, 1, 1), (GATE_UP, 1, 0, 2, 1), (DOWN, 1, 0, 3, 1),
-    (BACK, 0, 3, 0, 3), (GATE_UP, 1, 1, 1, 1), (EXCHANGE, 2, 0, 2, 0), (DOWN, 1, 1, 2, 1),
-    (GATE_UP, 2, 0, 2, 0), (COMBINE, 1, 0, 3, 1), (DOWN, 2, 0, 2, 0), (BACK, 1, 0, 1, 0),
-    (COMBINE, 3, 1, 0, 0), (GATE_UP, 2, 1, 3, 0), (BACK, 1, 1, 1, 1), (COMBINE, 2, 0, 2, 1),
-    (BACK, 2, 1, 3, 3), (DOWN, 3, 0, 1, 1), (DOWN, 2, 1, 3, 0), (BACK, 2, 0, 0, 0),
-    (COMBINE, 1, 1, 2, 0), (BACK, 1, 2, 2, 1), (BACK, 3, 3, 2, 0), (BACK, 1, 3, 2, 2),
-    (COMBINE, 2, 1, 1, 1), (BACK, 2, 2, 3, 2), (BACK, 3, 2, 2, 3), (BACK, 2, 3, 1, 2),
-    (BACK, 0, 1, 1, 3), (COMBINE, 3, 0, 3, 0), (BACK, 3, 1, 3, 1), (BACK, 3, 0, 3, 0),
+    (SEND, 1, 0, 0, 0), (SEND, 3, 0, 1, 0), (SEND, 0, 0, 3, 0), (METAS, 0, 0, 0, 0),
+    (ARRIVE, 0, 1, 0, 0), (ARRIVE, 3, 0, 0, 2), (ARRIVE, 3, 3, 0, 3), (SELECT, 0, 0, 0, 0),
+    (ARRIVE, 3, 2, 3, 2), (ARRIVE, 0, 2, 3, 3), (EXCHANGE, 0, 0, 0, 0), (SEND, 2, 0, 2, 0),
+    (SELECT, 3, 1, 0, 1), (ARRIVE, 0, 3, 1, 1), (WAIT_W, 0, 0, 0, 0), (GATE_UP, 0, 0, 0, 0),
+    (SELECT, 0, 1, 3, 1), (DOWN, 0, 0, 0, 0), (ARRIVE, 2, 3, 3, 0), (ARRIVE, 3, 1, 1, 0),
+    (EXCHANGE, 0, 1, 0, 1), (ARRIVE, 1, 1, 2, 3), (ARRIVE, 2, 2, 3, 1), (SELECT, 2, 1, 1, 0),
+    (ARRIVE, 1, 0, 1, 3), (GATE_UP, 0, 1, 0, 1), (DOWN, 0, 1, 0, 1), (ARRIVE, 1, 3, 2, 0),
+    (ARRIVE, 2, 0, 2, 2), (SELECT, 1, 0, 2, 1), (ARRIVE, 2, 1, 2, 1), (SELECT, 2, 0, 2, 0),
+    (ARRIVE, 1, 2, 1, 2), (EXCHANGE, 1, 0, 2, 0), (SELECT, 1, 1, 1, 1), (EXCHANGE, 2, 1, 1, 0),
+    (EXCHANGE, 3, 1, 3, 1), (COMBINE, 0, 1, 0, 1), (COMBINE, 0, 0, 0, 0), (GATE_UP, 1, 0, 2, 0),
+    (SELECT, 3, 0, 3, 0), (BACK, 0, 3, 0, 3), (GATE_UP, 3, 1, 1, 0), (EXCHANGE, 1, 1, 1, 1),
+    (DOWN, 1, 0, 2, 0), (EXCHANGE, 2, 0, 2, 1), (GATE_UP, 1, 1, 3, 1), (EXCHANGE, 3, 0, 3, 0),
+    (DOWN, 3, 1, 1, 0), (BACK, 0, 2, 0, 2), (GATE_UP, 2, 0, 1, 1), (DOWN, 2, 0, 3, 1),
+    (COMBINE, 1, 0, 2, 0), (BACK, 1, 0, 0, 0), (GATE_UP, 2, 1, 2, 1), (COMBINE, 3, 1, 1, 0),
+    (DOWN, 2, 1, 2, 1), (BACK, 1, 1, 1, 0), (GATE_UP, 3, 0, 3, 0), (COMBINE, 2, 0, 3, 1),
+    (DOWN, 1, 1, 1, 1), (BACK, 2, 1, 2, 1), (BACK, 2, 0, 3, 3), (COMBINE, 1, 1, 2, 1),
+    (BACK, 1, 3, 1, 1), (BACK, 1, 2, 2, 0), (BACK, 3, 3, 2, 2), (DOWN, 3, 0, 3, 0),
+    (COMBINE, 2, 1, 1, 1), (BACK, 2, 2, 3, 2), (BACK, 3, 2, 2, 3), (COMBINE, 3, 0, 3, 0),
+    (BACK, 2, 3, 1, 2), (BACK, 0, 1, 1, 3), (BACK, 3, 1, 3, 1), (BACK, 3, 0, 3, 0),
 )
 
 

time: 139 us -> 146 us (1.050)
  Pallas kernels: 137 us -> 144 us
    pallas_call x1, Pallas kernels: 137 us -> 144 us  [body(): pl.pallas_call(functools.partial(kernel, cfg), out_shape=jax.ShapeDtypeSt...]
where the time goes in v6:
time: 146 us
  Pallas kernels  144 us (99%)
  local copies, waits for them, and re-layouts  1.67 us (1%)
    pallas_call x1, Pallas kernels, body(): pl.pallas_call(functools.partial(kernel, cfg), out_shape=jax.ShapeDtypeSt...  144 us

profile of v6, /device:TPU:33, one launch (start us, length us, event | category | flops | bytes accessed | tf_op | source)
XLA Modules:
  0.0 146.1 jit_solution(7239864578233408811)
XLA Ops:
  0.0 144.4 %shard_map.82 = bf16[128,1024]{1,0:T(8,128)(2,1)} custom-call(s32[4,128]{1,0:T(4,128)} %bitcast.6, f32[4,128]{1,0:T(4,128)} %bitcast.7, bf16[128,2048]{1,0:T(8,128)(2,1)} %tokens.1, f32[1,2048]{1,0:T(1,128)} %bitcast.4, f32[1,1024]{1,0:T(1,128)} %bitcast.5, bf16[2,2048,256]{2,1,0:T(8,128)(2,1)} %wg_hbm.1, bf16[2,2048,256]{2,1,0:T(8,128)(2,1)} %wu_hbm.1, ...), custom_call_target="tpu_custom_call" | custom-call | tf_op jit(solution)/shard_map/pallas_call | solution.py:499
  144.4 1.7 %copy.10 = bf16[128,1024]{1,0:T(8,128)(2,1)} copy(bf16[128,1024]{1,0:T(8,128)(2,1)} %shard_map.82) | data formatting | bytes 524288

commit v7 on v6

--- a/solution.py
+++ b/solution.py
@@ -28,29 +28,29 @@
     return lax.dot_general(a, b, (((0,), (0,)), ((), ())), preferred_element_type=F32)
 
 
-PARTS = 4
+PARTS = 2
 ARRIVE, BACK, SELECT, EXCHANGE, GATE_UP, DOWN, COMBINE, SEND, METAS, WAIT_W = range(10)
 
 PLAN = (
     (SEND, 1, 0, 0, 0), (SEND, 3, 0, 1, 0), (SEND, 0, 0, 3, 0), (METAS, 0, 0, 0, 0),
-    (ARRIVE, 0, 1, 0, 0), (ARRIVE, 3, 0, 0, 2), (ARRIVE, 3, 3, 0, 3), (SELECT, 0, 0, 0, 0),
-    (ARRIVE, 3, 2, 3, 2), (ARRIVE, 0, 2, 3, 3), (EXCHANGE, 0, 0, 0, 0), (SEND, 2, 0, 2, 0),
-    (SELECT, 3, 1, 0, 1), (ARRIVE, 0, 3, 1, 1), (WAIT_W, 0, 0, 0, 0), (GATE_UP, 0, 0, 0, 0),
-    (SELECT, 0, 1, 3, 1), (DOWN, 0, 0, 0, 0), (ARRIVE, 2, 3, 3, 0), (ARRIVE, 3, 1, 1, 0),
-    (EXCHANGE, 0, 1, 0, 1), (ARRIVE, 1, 1, 2, 3), (ARRIVE, 2, 2, 3, 1), (SELECT, 2, 1, 1, 0),
-    (ARRIVE, 1, 0, 1, 3), (GATE_UP, 0, 1, 0, 1), (DOWN, 0, 1, 0, 1), (ARRIVE, 1, 3, 2, 0),
-    (ARRIVE, 2, 0, 2, 2), (SELECT, 1, 0, 2, 1), (ARRIVE, 2, 1, 2, 1), (SELECT, 2, 0, 2, 0),
-    (ARRIVE, 1, 2, 1, 2), (EXCHANGE, 1, 0, 2, 0), (SELECT, 1, 1, 1, 1), (EXCHANGE, 2, 1, 1, 0),
-    (EXCHANGE, 3, 1, 3, 1), (COMBINE, 0, 1, 0, 1), (COMBINE, 0, 0, 0, 0), (GATE_UP, 1, 0, 2, 0),
-    (SELECT, 3, 0, 3, 0), (BACK, 0, 3, 0, 3), (GATE_UP, 3, 1, 1, 0), (EXCHANGE, 1, 1, 1, 1),
-    (DOWN, 1, 0, 2, 0), (EXCHANGE, 2, 0, 2, 1), (GATE_UP, 1, 1, 3, 1), (EXCHANGE, 3, 0, 3, 0),
-    (DOWN, 3, 1, 1, 0), (BACK, 0, 2, 0, 2), (GATE_UP, 2, 0, 1, 1), (DOWN, 2, 0, 3, 1),
-    (COMBINE, 1, 0, 2, 0), (BACK, 1, 0, 0, 0), (GATE_UP, 2, 1, 2, 1), (COMBINE, 3, 1, 1, 0),
-    (DOWN, 2, 1, 2, 1), (BACK, 1, 1, 1, 0), (GATE_UP, 3, 0, 3, 0), (COMBINE, 2, 0, 3, 1),
-    (DOWN, 1, 1, 1, 1), (BACK, 2, 1, 2, 1), (BACK, 2, 0, 3, 3), (COMBINE, 1, 1, 2, 1),
-    (BACK, 1, 3, 1, 1), (BACK, 1, 2, 2, 0), (BACK, 3, 3, 2, 2), (DOWN, 3, 0, 3, 0),
-    (COMBINE, 2, 1, 1, 1), (BACK, 2, 2, 3, 2), (BACK, 3, 2, 2, 3), (COMBINE, 3, 0, 3, 0),
-    (BACK, 2, 3, 1, 2), (BACK, 0, 1, 1, 3), (BACK, 3, 1, 3, 1), (BACK, 3, 0, 3, 0),
+    (ARRIVE, 0, 1, 0, 2), (ARRIVE, 3, 3, 0, 0), (SELECT, 0, 0, 0, 0), (ARRIVE, 3, 0, 0, 3),
+    (ARRIVE, 3, 2, 3, 0), (EXCHANGE, 0, 0, 0, 0), (SELECT, 3, 1, 0, 1), (SEND, 2, 0, 2, 0),
+    (ARRIVE, 0, 2, 3, 3), (WAIT_W, 0, 0, 0, 0), (GATE_UP, 0, 0, 0, 0), (DOWN, 0, 0, 0, 0),
+    (ARRIVE, 0, 3, 3, 2), (ARRIVE, 2, 3, 1, 0), (SELECT, 0, 1, 3, 1), (ARRIVE, 3, 1, 2, 3),
+    (EXCHANGE, 0, 1, 0, 1), (COMBINE, 0, 0, 0, 0), (ARRIVE, 2, 2, 1, 1), (SELECT, 2, 1, 1, 0),
+    (ARRIVE, 1, 0, 3, 1), (ARRIVE, 1, 1, 1, 3), (GATE_UP, 0, 1, 0, 1), (DOWN, 0, 1, 0, 1),
+    (EXCHANGE, 2, 1, 3, 1), (ARRIVE, 1, 3, 2, 0), (ARRIVE, 2, 0, 2, 2), (SELECT, 1, 0, 3, 0),
+    (ARRIVE, 2, 1, 2, 1), (EXCHANGE, 3, 1, 1, 0), (SELECT, 2, 0, 2, 0), (ARRIVE, 1, 2, 1, 2),
+    (EXCHANGE, 1, 0, 2, 0), (SELECT, 1, 1, 2, 1), (GATE_UP, 3, 1, 1, 0), (EXCHANGE, 2, 0, 3, 0),
+    (SELECT, 3, 0, 1, 1), (COMBINE, 0, 1, 0, 1), (BACK, 0, 3, 0, 3), (GATE_UP, 1, 0, 2, 0),
+    (DOWN, 1, 0, 1, 0), (GATE_UP, 2, 1, 3, 1), (EXCHANGE, 1, 1, 1, 1), (BACK, 0, 2, 0, 2),
+    (EXCHANGE, 3, 0, 2, 1), (DOWN, 3, 1, 2, 0), (GATE_UP, 2, 0, 2, 1), (DOWN, 2, 0, 3, 1),
+    (COMBINE, 1, 0, 1, 0), (BACK, 1, 0, 1, 0), (BACK, 1, 1, 0, 0), (GATE_UP, 1, 1, 3, 0),
+    (GATE_UP, 3, 0, 1, 1), (DOWN, 1, 1, 2, 1), (COMBINE, 2, 0, 2, 0), (BACK, 2, 1, 1, 1),
+    (COMBINE, 1, 1, 3, 1), (BACK, 2, 0, 2, 1), (BACK, 1, 2, 3, 3), (DOWN, 2, 1, 1, 1),
+    (COMBINE, 3, 1, 2, 1), (BACK, 1, 3, 2, 0), (BACK, 3, 3, 2, 2), (DOWN, 3, 0, 3, 0),
+    (COMBINE, 2, 1, 1, 1), (BACK, 2, 2, 3, 2), (COMBINE, 3, 0, 3, 0), (BACK, 3, 2, 1, 2),
+    (BACK, 2, 3, 1, 3), (BACK, 0, 1, 2, 3), (BACK, 3, 1, 3, 1), (BACK, 3, 0, 3, 0),
 )
 
 

time: 146 us -> 148 us (1.014)
  Pallas kernels: 144 us -> 146 us
where the time goes in v7:
time: 148 us; the launch traced here: 147 us
  Pallas kernels  146 us (99%)
  local copies, waits for them, and re-layouts  1.67 us (1%)
    pallas_call x1, Pallas kernels, body(): pl.pallas_call(functools.partial(kernel, cfg), out_shape=jax.ShapeDtypeSt...  146 us

profile of v7, /device:TPU:33, one launch (start us, length us, event | category | flops | bytes accessed | tf_op | source)
XLA Modules:
  0.0 147.5 jit_solution(807776612201849238)
XLA Ops:
  0.0 145.8 %shard_map.82 = bf16[128,1024]{1,0:T(8,128)(2,1)} custom-call(s32[4,128]{1,0:T(4,128)} %bitcast.6, f32[4,128]{1,0:T(4,128)} %bitcast.7, bf16[128,2048]{1,0:T(8,128)(2,1)} %tokens.1, f32[1,2048]{1,0:T(1,128)} %bitcast.4, f32[1,1024]{1,0:T(1,128)} %bitcast.5, bf16[2,2048,256]{2,1,0:T(8,128)(2,1)} %wg_hbm.1, bf16[2,2048,256]{2,1,0:T(8,128)(2,1)} %wu_hbm.1, ...), custom_call_target="tpu_custom_call" | custom-call | tf_op jit(solution)/shard_map/pallas_call | solution.py:499
  145.8 1.7 %copy.10 = bf16[128,1024]{1,0:T(8,128)(2,1)} copy(bf16[128,1024]{1,0:T(8,128)(2,1)} %shard_map.82) | data formatting | bytes 524288
